TPU v7x, 128 devices: a whole 4x4x4 slice. The times are simulated.
128 devices in a mesh: sp: 8 (over x, core), tp: 16 (over z, y).
Axes of the slice: x: 4, y: 4, z: 4, core: 2. Of those that a mesh axis runs over, the one named last changes fastest.
Arguments:
- tokens: bfloat16 [4, 2048, 2048], P(None, ('sp', 'tp')), may hold values from -6 to 6
- norm_gain: float32 [2048], replicated, may hold values from 0.5 to 1.5
- entry_projection: bfloat16 [2048, 2048], P(None, 'tp'), may hold values from -0.125 to 0.125
- valve_projection: bfloat16 [2048, 2048], P(None, 'tp'), may hold values from -0.125 to 0.125
- filter_taps: float32 [4, 2048], P(None, 'tp'), may hold values from -3 to 3
- conv_bias: float32 [2048], P('tp'), may hold values from -0.6 to 0.6
- recur_weight: bfloat16 [16, 128, 128], P('tp'), may hold values from -0.5 to 0.5
- recur_bias: float32 [2048], P('tp'), may hold values from -3 to 3
- entry_weight: bfloat16 [16, 128, 128], P('tp'), may hold values from -0.5 to 0.5
- entry_bias: float32 [2048], P('tp'), may hold values from -0.6 to 0.6
- forget_rate: float32 [2048], P('tp'), may hold values from 3.0517578e-05 to 0.25, as said below
- output_weight: bfloat16 [2048, 2048], P('tp'), may hold values from -0.5 to 0.5
Outputs:
- mixed: bfloat16 [4, 2048, 2048], P(None, ('sp', 'tp'))
Inputs may be any that keep to these rules, and one draw needn't show every extreme that they name: forget_rate is positive; its even channels lie between 1 / 32768 and 1 / 8192, its odd channels between 1 / 64 and 1 / 4.
All inputs are finite; a program needn't handle non-finite values.
Results may differ from a plain program's by a relative error of at most 0.02.
Values may be sent and summed in bfloat16 or wider, within the bound.
A program may use at most 64 MiB of HBM per device.

v0:
```python
import jax
import jax.numpy as jnp
from jax import lax
from jax.sharding import Mesh
from jax.sharding import PartitionSpec as P

TP = ("tp_0", "tp_1")
SP_TP = ("sp", "tp_0", "tp_1")


epsilon = 1e-06
gate_power = 8.0


def over_all(shard, axis, dim, work):
    return work(lax.all_gather(shard, axis, axis=dim, tiled=True), jnp.int32(0))


def from_behind(value, axis, by):
    devices = lax.axis_size(axis)
    pairs = [(i, i + by) for i in range(devices) if 0 <= i + by < devices]
    return lax.ppermute(value, axis, pairs)


def entering_2(part, axis, combine, identity, reverse):
    count = lax.axis_size(axis)
    place = lax.axis_index(axis)
    ahead = count - 1 - place if reverse else place
    gathered = jax.tree.map(lambda a: lax.all_gather(a, axis), part)
    state = jax.tree.map(lambda a, e: jnp.zeros_like(a) + jnp.asarray(e, a.dtype), part, identity)

    def one(hop, state):
        source = count - 1 - hop if reverse else hop
        return combine(
            state, jax.tree.map(lambda a: lax.dynamic_index_in_dim(a, source, 0, False), gathered)
        )

    return lax.fori_loop(0, ahead, one, state)


def sum_by_axis(product, rows, axes):
    running = product(jnp.int32(0), rows * lax.axis_size(axes)).astype(jnp.bfloat16)
    for axis in axes:
        running = lax.psum_scatter(running, axis, scatter_dimension=0, tiled=True)
    return running.astype(jnp.float32)


def combine_pair(earlier, latter):
    return (earlier[0] * latter[0], latter[0] * earlier[1] + latter[1])


def block_product(convolved, weight):
    blocks = weight.shape[0]
    block_width = weight.shape[1]
    grouped = convolved.reshape(convolved.shape[0], convolved.shape[1], blocks, block_width)
    product = jnp.einsum("slhi,hij->slhj", grouped, weight, preferred_element_type=jnp.float32)
    return product.reshape(convolved.shape)


def per_device(
    tokens,
    norm_gain,
    entry_projection,
    valve_projection,
    filter_taps,
    conv_bias,
    recur_weight,
    recur_bias,
    entry_weight,
    entry_bias,
    forget_rate,
    output_weight,
):
    widened = tokens.astype(jnp.float32)
    scaled = widened * lax.rsqrt(jnp.mean(widened * widened, axis=-1, keepdims=True) + epsilon)
    rescaled_values = (scaled * norm_gain).astype(jnp.bfloat16)
    channels = entry_projection.shape[1]

    def project(partition_lines, row_start):
        input_part = jnp.einsum(
            "tgy,yu->tgu", partition_lines, entry_projection, preferred_element_type=jnp.float32
        )
        gate_part = jnp.einsum(
            "tgy,yu->tgu", partition_lines, valve_projection, preferred_element_type=jnp.float32
        )
        return jnp.concatenate(
            [input_part.astype(jnp.bfloat16), gate_part.astype(jnp.bfloat16)], axis=-1
        )

    projected = over_all(rescaled_values, TP, 1, project)
    conv_input = projected[:, :, :channels]
    gate_logits = projected[:, :, channels:]
    conv_width = filter_taps.shape[0]
    length = conv_input.shape[1]
    before = from_behind(conv_input[:, length - (conv_width - 1) :, :], "sp", 1)
    padded = jnp.concatenate([before, conv_input], axis=1).astype(jnp.float32)
    summed = conv_bias + padded[:, 0:length] * filter_taps[0]
    for offset in range(1, conv_width):
        summed = summed + padded[:, offset : offset + length] * filter_taps[offset]
    convolved = summed.astype(jnp.bfloat16)
    recur_gate = jax.nn.sigmoid(block_product(convolved, recur_weight) + recur_bias)
    entry_gate = jax.nn.sigmoid(block_product(convolved, entry_weight) + entry_bias)
    log_decay = -gate_power * recur_gate * forget_rate
    decay = jnp.exp(log_decay)
    pushed = jnp.sqrt(-jnp.expm1(2.0 * log_decay)) * (entry_gate * convolved.astype(jnp.float32))
    running = jnp.cumsum(log_decay, axis=1)
    total_log = running[:, -1]
    stretch_decay = jnp.exp(total_log)
    stretch_state = jnp.sum(pushed * jnp.exp(total_log[:, None] - running), axis=1)
    unchanged_passthrough = (jnp.ones_like(stretch_decay), jnp.zeros_like(stretch_state))
    entering = entering_2(
        (stretch_decay, stretch_state), "sp", combine_pair, unchanged_passthrough, False
    )[1]
    seeded = jnp.concatenate(
        [pushed[:, :1] + decay[:, :1] * entering[:, None], pushed[:, 1:]], axis=1
    )
    hidden_state = lax.associative_scan(combine_pair, (decay, seeded), axis=1)[1]
    valved_lines = (hidden_state * jax.nn.silu(gate_logits.astype(jnp.float32))).astype(
        jnp.bfloat16
    )
    kept_rows = length // lax.axis_size(TP)

    def output_term(row_start, row_count):
        segment = lax.dynamic_slice_in_dim(valved_lines, row_start, row_count, 1)
        return jnp.einsum("slc,cd->lsd", segment, output_weight, preferred_element_type=jnp.float32)

    mixed_rows = sum_by_axis(output_term, kept_rows, TP)
    return jnp.transpose(mixed_rows.astype(jnp.bfloat16), (1, 0, 2))


def solution(mesh):
    finer = Mesh(mesh.devices.reshape(mesh.shape["sp"], 4, 4), ("sp", "tp_0", "tp_1"))
    placed = (
        P(None, SP_TP, None),
        P(),
        P(None, TP),
        P(None, TP),
        P(None, TP),
        P(TP),
        P(TP, None, None),
        P(TP),
        P(TP, None, None),
        P(TP),
        P(TP),
        P(TP, None),
    )
    return jax.shard_map(
        per_device, mesh=finer, in_specs=placed, out_specs=P(None, SP_TP, None), check_vma=False
    )
```

profile of v0, /device:TPU:1, one launch (start us, length us, event | category | flops | bytes accessed | tf_op | source)
XLA Modules:
  0.0 189.0 jit_solution(3632505429741346802)
XLA Ops:
  6.5 1.1 fusion.12
  7.7 1.8 fusion.14
  9.6 0.8 slice_bitcast_fusion.4
  10.4 53.5 %all-gather.5.cloned.1.call-done = bf16[4,256,2048]{2,1,0:T(8,128)(2,1)} async-done(((bf16[4,16,2048]{2,1,0:T(8,128)(2,1)}), bf16[4,256,2048]{2,1,0:T(8,128)(2,1)}) %all-gather.5.cloned.1.call-update) | async-done | bytes 4194320 | tf_op jit(solution)/shard_map/all_gather | solution.py:16
  63.9 3.5 %convolution_convert_fusion.1 = bf16[4,256,128]{2,1,0:T(8,128)(2,1)S(1)} fusion(bf16[4,256,2048]{2,1,0:T(8,128)(2,1)} %all-gather.5.cloned.1.call-done, bf16[2048,128]{1,0:T(8,128)(2,1)} %param.16), kind=kOutput, calls=%fused_computation.18 | convolution fusion | flops 537001984 | bytes 4980736 | tf_op jit(solution)/shard_map/tgy,yu->tgu/dot_general | solution.py:80
  67.5 4.1 %collective-permute-start = (bf16[4,3,128]{2,1,0:T(4,128)(2,1)S(1)}, bf16[4,3,128]{2,1,0:T(4,128)(2,1)S(1)}, u32[]{:S(2)}, u32[]{:S(2)}) collective-permute-start(bf16[4,3,128]{2,1,0:T(4,128)(2,1)S(1)} %slice.298), channel_id=1, source_target_pairs={{0,16},{16,32},{32,48},{48,64},{64,80},{80,96},{96,112},{1,17},{17... | collective-permute-start | bytes 9224 | tf_op jit(solution)/shard_map/ppermute | solution.py:22
  71.6 0.7 collective-permute-done
  72.4 0.3 fusion.16
  72.7 0.4 fusion.53
  73.1 0.1 slice.245
  73.2 0.1 slice.240
  73.3 0.1 slice.239
  73.4 0.4 fusion.23
  73.9 0.2 broadcast_add_fusion
  74.2 0.6 multiply_reduce_fusion
  74.8 0.1 slice.297
  75.0 0.1 slice.243
  75.1 14.0 %all-gather.2 = f32[8,4,128]{2,1,0:T(4,128)S(1)} all-gather(f32[1,4,128]{2,1,0:T(4,128)S(1)} %bitcast.91), channel_id=3, replica_groups=mesh['sp'=8,'tp_0'=4,'tp_1'=4] {'sp'}, dimensions={0}, use_global_device_ids=true | all-gather | bytes 18432 | tf_op jit(solution)/shard_map/all_gather | solution.py:29
  89.1 12.7 %all-gather = f32[32,1,128]{2,1,0:T(1,128)S(1)} all-gather(f32[4,1,128]{2,1,0:T(1,128)S(1)} %get-tuple-element.61), channel_id=2, replica_groups=mesh['sp'=8,'tp_0'=4,'tp_1'=4] {'sp'}, dimensions={0}, use_global_device_ids=true | all-gather | bytes 18432 | tf_op jit(solution)/shard_map/all_gather | solution.py:29
  101.8 0.1 slice.242
  104.2 0.1 pad.64
  104.3 8.5 %convert_bitcast_fusion = bf16[256,4,2048]{2,0,1:T(8,128)(2,1)} fusion(bf16[128,2048]{1,0:T(8,128)(2,1)S(1)} %copy-done, bf16[4,256,2048]{2,1,0:T(8,128)(2,1)} %all-gather.5.cloned.1.call-done, bf16[2048,128]{1,0:T(8,128)(2,1)S(1)} %copy-done.1, f32[4,256,128]{2,1,0:T(8,128)S(1)} %pad.63, f32[4,256,128]{2,1,0:T(8,128)S(1)} %pad.64), kind=kOutput, calls=%fused_computation.2 | convolution fusion | flops 1077018624 | bytes 10485760 | tf_op jit(solution)/shard_map/slc,cd->lsd/dot_general | solution.py:125
  112.9 45.4 %reduce-scatter.3.cloned.1.call-done = bf16[64,4,2048]{2,0,1:T(8,128)(2,1)} async-done(((bf16[256,4,2048]{2,0,1:T(8,128)(2,1)}), bf16[64,4,2048]{2,0,1:T(8,128)(2,1)}) %reduce-scatter.3.cloned.1.call-update) | async-done | bytes 1048592 | tf_op jit(solution)/shard_map/reduce_scatter | solution.py:44
  158.3 24.2 %reduce-scatter.5.cloned.1.call-done = bf16[16,4,2048]{2,0,1:T(8,128)(2,1)} async-done(((bf16[64,4,2048]{2,0,1:T(8,128)(2,1)}), bf16[16,4,2048]{2,0,1:T(8,128)(2,1)}) %reduce-scatter.5.cloned.1.call-update) | async-done | bytes 262160 | tf_op jit(solution)/shard_map/reduce_scatter | solution.py:44
  (118 shorter events, 2.2 us)
Async XLA Ops:
  6.5 97.7 %copy-start = (bf16[128,2048]{1,0:T(8,128)(2,1)S(1)}, bf16[128,2048]{1,0:T(8,128)(2,1)}, u32[]{:S(2)}) copy-start(bf16[128,2048]{1,0:T(8,128)(2,1)} %param.25) | copy-start | bytes 1572868
  6.5 57.4 %all-gather.5.cloned.1.call-start = ((), (), s32[]{:S(2)}) async-start(), calls=%async_computation.2 | async-start | bytes 4456448 | tf_op jit(solution)/shard_map/all_gather | solution.py:16
  7.7 63.9 %copy-start.5 = (f32[128]{0:T(128)S(1)}, f32[128]{0:T(128)}, u32[]{:S(2)}) copy-start(f32[128]{0:T(128)} %param.24) | copy-start | bytes 1540
  9.5 148.7 %reduce-scatter.3.cloned.1.call-start = ((), (), s32[]{:S(2)}) async-start(), calls=%async_computation.3 | async-start | bytes 5242880 | tf_op jit(solution)/shard_map/reduce_scatter | solution.py:44
  10.4 62.0 %copy-start.2 = (f32[128]{0:T(128)S(1)}, f32[128]{0:T(128)}, u32[]{:S(2)}) copy-start(f32[128]{0:T(128)} %param.19) | copy-start | bytes 1540
  10.4 62.2 %copy-start.3 = (bf16[1,128,128]{2,1,0:T(8,128)(2,1)S(1)}, bf16[1,128,128]{2,1,0:T(8,128)(2,1)}, u32[]{:S(2)}) copy-start(bf16[1,128,128]{2,1,0:T(8,128)(2,1)} %param.20) | copy-start | bytes 98308
  10.4 62.2 %copy-start.6 = (f32[128]{0:T(128)S(1)}, f32[128]{0:T(128)}, u32[]{:S(2)}) copy-start(f32[128]{0:T(128)} %param.21) | copy-start | bytes 1540
  67.5 4.8 %collective-permute-start = (bf16[4,3,128]{2,1,0:T(4,128)(2,1)S(1)}, bf16[4,3,128]{2,1,0:T(4,128)(2,1)S(1)}, u32[]{:S(2)}, u32[]{:S(2)}) collective-permute-start(bf16[4,3,128]{2,1,0:T(4,128)(2,1)S(1)} %slice.298), channel_id=1, source_target_pairs={{0,16},{16,32},{32,48},{48,64},{64,80},{80,96},{96,112},{1,17},{17... | collective-permute-start | bytes 9224 | tf_op jit(solution)/shard_map/ppermute | solution.py:22
  72.7 1.5 copy-start.4
  72.7 1.5 copy-start.7
  103.0 1.3 copy-start.1
  112.8 69.6 %reduce-scatter.5.cloned.1.call-start = ((), (), s32[]{:S(2)}) async-start(), calls=%async_computation.4 | async-start | bytes 1310720 | tf_op jit(solution)/shard_map/reduce_scatter | solution.py:44
Sparse Core Ops, SparseCore 0:
  9.6 54.2 all-gather.4
  113.0 45.2 reduce-scatter.2
  160.7 21.7 reduce-scatter.4
where the time goes:
time: 190 us; the launch traced here: 189 us
  waiting for transfers between devices  124 us (65%)
  blocking collectives  26.7 us (14%)
  between operations  13.8 us (7%)
  matrix products  13 us (7%)
  other arithmetic  4.47 us (2%)
  starting transfers between devices  4.19 us (2%)
  local copies, waits for them, and re-layouts  3.05 us (2%)
    reduce_scatter x2, waiting for transfers between devices, sum_by_axis(): running = lax.psum_scatter(running, axis, scatter_dimension=0, tiled=True)  69.6 us
    all_gather x1, waiting for transfers between devices, over_all(): return work(lax.all_gather(shard, axis, axis=dim, tiled=True), jnp.int32(0))  53.5 us
    all_gather x2, blocking collectives, entering_2(): gathered = jax.tree.map(lambda a: lax.all_gather(a, axis), part)  26.7 us
    dot_general x1, matrix products, output_term(): jnp.einsum('slc,cd->lsd', segment, output_weight, preferred_element_type=...  8.52 us
    ppermute x1, starting transfers between devices, from_behind(): return lax.ppermute(value, axis, pairs)  4.1 us
  transfers between devices with their start and end apart: 4, of which 4 were waited for; matrix products, arithmetic and copies ran while one was open for 0% of the time, Pallas kernels for 0%

commit v1 on v0

v1 whole, which is shorter than its diff:
```python
import jax
import jax.numpy as jnp
from jax import lax
from jax.experimental import pallas as pl
from jax.experimental.pallas import tpu as pltpu
from jax.sharding import Mesh
from jax.sharding import PartitionSpec as P

MESH = pl.DeviceIdType.MESH
EPS = 1e-06
POWER = 8.0
SEQS = 4
TOK = 16
STR = 64
D = 2048
W = 128
NB = 4
CH = NB * W
ROWS = SEQS * STR
AROWS = D + 2 * W
PIECE = (AROWS // 8, D // 8, W // 8)
f32 = jnp.float32
bf16 = jnp.bfloat16


class Slots:
    def __init__(self):
        self.index = {}

    def __call__(self, *key):
        return self.index.setdefault(key, len(self.index))


N_COPIES = 104
N_LOCAL = 16


def neg_expm1(t):
    s = 1.0 + t * (1.0 / 8.0)
    for n in (7.0, 6.0, 5.0, 4.0, 3.0, 2.0):
        s = 1.0 + t * (1.0 / n) * s
    return jnp.where(t > -0.5, -t * s, 1.0 - jnp.exp(t))


def sigmoid(v):
    return 1.0 / (1.0 + jnp.exp(-v))


def kernel(
    tok_ref,
    gain_ref,
    w1_ref,
    w2_ref,
    rw_ref,
    ew_ref,
    small_ref,
    wo_ref,
    out_ref,
    tr,
    nt,
    wa,
    wv,
    wog,
    sm,
    ci,
    hs,
    hr,
    cv,
    lg,
    pc,
    hc,
    sg,
    gt,
    g16,
    s_own,
    l1,
    t_own,
    l2,
    pb,
    pf,
    rd,
    rb,
    ssem,
    rsem,
    lsem,
):
    X = lax.axis_index("x")
    C = lax.axis_index("c")
    Z = lax.axis_index("z")
    Y = lax.axis_index("y")
    g = X * 2 + C
    par = lax.rem(X, 2)

    def mod4(v):
        return lax.rem(v + 8, 4)

    def gdev(v):
        return {"x": v // 2, "c": lax.rem(v, 2)}

    nxt_z = mod4(Z + 1)
    nxt_g = lax.rem(g + jnp.where(Z == 3, 1, 0), 8)
    prv_z = mod4(Z - 1)
    prv_g = lax.rem(g + 8 - jnp.where(Z == 0, 1, 0), 8)
    nxt = {"x": nxt_g // 2, "c": lax.rem(nxt_g, 2), "z": nxt_z}
    prv = {"x": prv_g // 2, "c": lax.rem(prv_g, 2), "z": prv_z}
    yp, ym = {"y": mod4(Y + 1)}, {"y": mod4(Y - 1)}
    zp, zm = {"z": nxt_z}, {"z": prv_z}
    xp, xm = {"x": mod4(X + 1)}, {"x": mod4(X - 1)}
    mate = {"c": 1 - C}

    slot = Slots()
    local = Slots()
    sent = []

    def send(key, src, dst, dev):
        k = slot(*key)
        copy = pltpu.make_async_remote_copy(
            src_ref=src,
            dst_ref=dst,
            send_sem=ssem.at[k],
            recv_sem=rsem.at[k],
            device_id=dev,
            device_id_type=MESH,
        )
        copy.start()
        sent.append(copy)

    def arrived(key, dst):
        k = slot(*key)
        pltpu.make_async_remote_copy(
            src_ref=dst,
            dst_ref=dst,
            send_sem=ssem.at[k],
            recv_sem=rsem.at[k],
            device_id=mate,
            device_id_type=MESH,
        ).wait_recv()

    def fetch(key, src, dst):
        copy = pltpu.make_async_copy(src, dst, lsem.at[local(key)])
        copy.start()
        return copy

    lanes = pl.ds(pl.multiple_of(Z * W, W), W)
    own_tok = tr.at[:, pl.ds(pl.multiple_of(Y * TOK, TOK), TOK), :]
    c_tok = fetch("tok", tok_ref, own_tok)
    c_wa = [
        fetch("w1", w1_ref, wa.at[pl.ds(0, D), lanes]),
        fetch("rw", rw_ref.at[0], wa.at[pl.ds(D, W), lanes]),
        fetch("ew", ew_ref.at[0], wa.at[pl.ds(D + W, W), lanes]),
    ]
    c_sm = fetch("small", small_ref, sm.at[Z])
    c_wv = fetch("w2", w2_ref, wv.at[:, lanes])
    c_wo = fetch("wo", wo_ref, wog.at[pl.ds(pl.multiple_of(Z * W, W), W), :])

    l2[...] = jnp.zeros_like(l2)

    barrier = pltpu.get_barrier_semaphore()
    partners = [yp, ym] + [{"z": mod4(Z + d)} for d in (1, 2, 3)]
    partners += [gdev(lax.rem(g + d, 8)) for d in range(1, 8)] + [nxt, prv]
    for dev in partners:
        pl.semaphore_signal(barrier, inc=1, device_id=dev, device_id_type=MESH)
    pl.semaphore_wait(barrier, len(partners))

    def tok(y, half):
        return tr.at[pl.ds(2 * half, 2), pl.ds(pl.multiple_of(y * TOK, TOK), TOK), :]

    y_m, y_p, y_d = mod4(Y - 1), mod4(Y + 1), mod4(Y + 2)
    c_tok.wait()
    send(("t", 0, 0), tok(Y, 0), tok(Y, 0), yp)
    send(("t", 1, 1), tok(Y, 1), tok(Y, 1), ym)
    send(("t", 0, 1), tok(Y, 1), tok(Y, 1), yp)
    send(("t", 1, 0), tok(Y, 0), tok(Y, 0), ym)

    def piece(m, z, q, core, h):
        rows = PIECE[m]
        k = q * 4 + core * 2 + h
        if m == 2:
            return wog.at[pl.ds(pl.multiple_of(z * W + k * rows, rows), rows), :]
        ref = (wa, wv)[m]
        return ref.at[pl.ds(pl.multiple_of(k * rows, rows), rows), pl.ds(pl.multiple_of(z * W, W), W)]

    blocks = (mod4(Z - 1), mod4(Z + 1), mod4(Z + 2))

    def own_send(m):
        for j, h, dev in ((0, 0, zp), (1, 1, zm), (0, 1, zp), (1, 0, zm)):
            ref = piece(m, Z, par, C, h)
            send(("z", m, j, h), ref, ref, dev)

    def z_event(m, j, h):
        ref = piece(m, blocks[j], par, C, h)
        arrived(("z", m, j, h), ref)
        if (j, h) == (0, 0):
            send(("z", m, 2, 0), ref, ref, zp)
        if (j, h) == (1, 1):
            send(("z", m, 2, 1), ref, ref, zm)
        send(("x", m, j, h), ref, ref, xp if h == 0 else xm)
        send(("d", m, j, 0, h), ref, ref, mate)

    def x_event(m, j, h):
        ref = piece(m, blocks[j], 1 - par, C, h)
        arrived(("x", m, j, h), ref)
        send(("d", m, j, 1, h), ref, ref, mate)

    def d_events(m):
        for j in range(3):
            for src in range(2):
                for h in range(2):
                    q = par if src == 0 else 1 - par
                    arrived(("d", m, j, src, h), piece(m, blocks[j], q, 1 - C, h))

    for c in c_wa:
        c.wait()
    own_send(0)
    c_sm.wait()
    for d in (1, 2, 3):
        send(("s", d), sm.at[Z], sm.at[Z], {"z": mod4(Z + d)})

    def norm(y, half):
        rows = pl.ds(pl.multiple_of(y * TOK, TOK), TOK)
        v = tr[pl.ds(2 * half, 2), rows, :].astype(f32)
        v = v * lax.rsqrt(jnp.mean(v * v, axis=-1, keepdims=True) + EPS)
        v = (v * gain_ref[...].reshape(1, 1, D)).astype(bf16)
        for s in range(2):
            nt[pl.ds(pl.multiple_of((2 * half + s) * STR + y * TOK, TOK), TOK), :] = v[s]

    norm(Y, 0)
    norm(Y, 1)
    z_event(0, 0, 0)
    z_event(0, 1, 1)
    c_wv.wait()
    own_send(1)
    arrived(("t", 0, 0), tok(y_m, 0))
    send(("t", 2, 0), tok(y_m, 0), tok(y_m, 0), yp)
    arrived(("t", 1, 1), tok(y_p, 1))
    send(("t", 2, 1), tok(y_p, 1), tok(y_p, 1), ym)
    z_event(0, 0, 1)
    z_event(0, 1, 0)
    norm(y_m, 0)
    norm(y_p, 1)
    z_event(0, 2, 0)
    z_event(0, 2, 1)
    x_event(0, 0, 0)
    x_event(0, 1, 1)
    z_event(1, 0, 0)
    z_event(1, 1, 1)
    c_wo.wait()
    own_send(2)
    x_event(0, 0, 1)
    x_event(0, 1, 0)
    arrived(("t", 0, 1), tok(y_m, 1))
    norm(y_m, 1)
    arrived(("t", 1, 0), tok(y_p, 0))
    norm(y_p, 0)
    z_event(1, 0, 1)
    z_event(1, 1, 0)
    x_event(0, 2, 0)
    x_event(0, 2, 1)
    arrived(("t", 2, 0), tok(y_d, 0))
    norm(y_d, 0)
    arrived(("t", 2, 1), tok(y_d, 1))
    norm(y_d, 1)
    z_event(1, 2, 0)
    z_event(1, 2, 1)
    x_event(1, 0, 0)
    x_event(1, 1, 1)
    d_events(0)

    conv_in = jnp.dot(nt[...], wa[0:D, :], preferred_element_type=f32).astype(bf16)
    for b in range(NB):
        part = conv_in[:, b * W : (b + 1) * W]
        ci[b] = part.astype(f32)
        for s in range(SEQS):
            hs[b, s * 8 : s * 8 + 8, :] = ci[b, s * STR + STR - 8 : s * STR + STR, :]
    send(("h",), hs, hr, nxt)
    for d in (1, 2, 3):
        arrived(("s", d), sm.at[mod4(Z - d)])
    x_event(1, 0, 1)
    x_event(1, 1, 0)
    z_event(2, 0, 0)
    z_event(2, 1, 1)
    x_event(1, 2, 0)
    x_event(1, 2, 1)
    arrived(("h",), hr)

    lane_row = lax.broadcasted_iota(jnp.int32, (8, W), 0)
    first = jnp.where(jnp.logical_and(g == 0, Z == 0), 0.0, 1.0).astype(f32)
    for b in range(NB):
        taps = [sm[b, k] for k in range(4)]
        bias = sm[b, 4]
        for s in range(SEQS):
            x = [ci[b, pl.ds(s * STR + i, 8, stride=8), :] for i in range(8)]
            behind = hr[b, s * 8 : s * 8 + 8, :] * first
            prev = {}
            for i in (5, 6, 7):
                prev[i - 8] = jnp.where(
                    lane_row == 0,
                    jnp.broadcast_to(behind[i : i + 1, :], (8, W)),
                    pltpu.roll(x[i], 1, 0),
                )
            rows = []
            for i in range(8):
                acc = jnp.broadcast_to(bias, (8, W))
                for k in range(4):
                    src = i - 3 + k
                    acc = acc + (x[src] if src >= 0 else prev[src]) * taps[k]
                rows.append(acc)
            cv[pl.ds(s * STR, STR), b * W : (b + 1) * W] = jnp.concatenate(rows, axis=0).astype(bf16)

    ends_a = [[None] * SEQS for _ in range(NB)]
    for b in range(NB):
        cols = slice(b * W, (b + 1) * W)
        block = cv[:, cols]
        lg[0] = jnp.dot(block, wa[D : D + W, cols], preferred_element_type=f32)
        lg[1] = jnp.dot(block, wa[D + W : D + 2 * W, cols], preferred_element_type=f32)
        r_bias, e_bias, rate = sm[b, 5], sm[b, 6], sm[b, 7]
        for s in range(SEQS):
            rows = slice(s * STR, (s + 1) * STR)
            r_gate = sigmoid(lg[0, rows, :] + r_bias)
            e_gate = sigmoid(lg[1, rows, :] + e_bias)
            log_decay = (-POWER * r_gate) * rate
            decay = jnp.exp(log_decay)
            pushed = jnp.sqrt(neg_expm1(2.0 * log_decay)) * (e_gate * cv[rows, cols].astype(f32))
            a = decay[0:8]
            h = pushed[0:8]
            pc[b, s * STR : s * STR + 8, :] = a
            hc[b, s * STR : s * STR + 8, :] = h
            for i in range(1, 8):
                step = decay[i * 8 : i * 8 + 8]
                h = step * h + pushed[i * 8 : i * 8 + 8]
                a = step * a
                pc[b, s * STR + i * 8 : s * STR + i * 8 + 8, :] = a
                hc[b, s * STR + i * 8 : s * STR + i * 8 + 8, :] = h
            for n in (1, 2, 4):
                keep = lane_row >= n
                a_in = jnp.where(keep, pltpu.roll(a, n, 0), 1.0)
                h_in = jnp.where(keep, pltpu.roll(h, n, 0), 0.0)
                h = a * h_in + h
                a = a * a_in
            s_own[s : s + 1, cols] = a[7:8]
            s_own[4 + s : 5 + s, cols] = h[7:8]
            ends_a[b][s] = (
                jnp.where(lane_row >= 1, pltpu.roll(a, 1, 0), 1.0),
                jnp.where(lane_row >= 1, pltpu.roll(h, 1, 0), 0.0),
            )

    for d in (1, 2, 3):
        send(("e", d), s_own, l1.at[Z], {"z": mod4(Z + d)})
    l1[Z] = s_own[...]
    z_event(2, 0, 1)
    z_event(2, 1, 0)
    x_event(2, 0, 0)
    x_event(2, 1, 1)
    for d in (1, 2, 3):
        arrived(("e", d), l1.at[mod4(Z - d)])
    total_a, total_h = l1[0, 0:4], l1[0, 4:8]
    for k in range(1, 4):
        ka, kh = l1[k, 0:4], l1[k, 4:8]
        total_h = ka * total_h + kh
        total_a = ka * total_a
    t_own[0:4] = total_a
    t_own[4:8] = total_h
    for d in range(1, 8):
        k = slot("g", d)

        @pl.when(g + d < 8)
        def _():
            pltpu.make_async_remote_copy(
                src_ref=t_own,
                dst_ref=l2.at[g],
                send_sem=ssem.at[k],
                recv_sem=rsem.at[k],
                device_id=gdev(lax.rem(g + d, 8)),
                device_id_type=MESH,
            ).start()

    z_event(2, 2, 0)
    z_event(2, 2, 1)
    d_events(1)
    x_event(2, 0, 1)
    x_event(2, 1, 0)
    logits = jnp.dot(nt[...], wv[...], preferred_element_type=f32).astype(bf16).astype(f32)
    for b in range(NB):
        v = logits[:, b * W : (b + 1) * W]
        sg[b] = v / (1.0 + jnp.exp(-v))
    x_event(2, 2, 0)
    x_event(2, 2, 1)
    for d in range(1, 8):
        k = slot("g", d)

        @pl.when(g - d >= 0)
        def _():
            ref = l2.at[lax.rem(g - d + 8, 8)]
            pltpu.make_async_remote_copy(
                src_ref=ref,
                dst_ref=ref,
                send_sem=ssem.at[k],
                recv_sem=rsem.at[k],
                device_id=mate,
                device_id_type=MESH,
            ).wait_recv()

    state = jnp.zeros((SEQS, CH), f32)
    for k in range(7):
        state = jnp.where(k < g, l2[k, 0:4] * state + l2[k, 4:8], state)
    for k in range(3):
        state = jnp.where(k < Z, l1[k, 0:4] * state + l1[k, 4:8], state)

    for b in range(NB):
        cols = slice(b * W, (b + 1) * W)
        for s in range(SEQS):
            chain_a, chain_h = ends_a[b][s]
            enter = chain_a * jnp.broadcast_to(state[s : s + 1, cols], (8, W)) + chain_h
            for i in range(8):
                at = s * STR + i * 8
                h = pc[b, at : at + 8, :] * enter + hc[b, at : at + 8, :]
                places = pl.ds(s * STR + i, 8, stride=8)
                gt[b, places, :] = h * sg[b, places, :]
        g16[:, cols] = gt[b].astype(bf16)

    d_events(2)

    def product(y):
        lhs = jnp.concatenate(
            [g16[pl.ds(pl.multiple_of(s * STR + y * TOK, TOK), TOK), :] for s in range(SEQS)], axis=0
        )
        return jnp.dot(lhs, wog[...], preferred_element_type=f32)

    p = product(y_d).astype(bf16).reshape(SEQS, TOK, D)
    pb[0] = p
    send(("r", 0), pb.at[0, pl.ds(0, 2)], rd.at[0], ym)
    send(("r", 1), pb.at[0, pl.ds(2, 2)], rd.at[1], yp)
    p = product(y_p).reshape(SEQS, TOK, D)
    pb[1, 0:2] = p[0:2].astype(bf16)
    send(("r", 2), pb.at[1, pl.ds(0, 2)], rb.at[0, pl.ds(0, 2)], yp)
    pf[1] = p[2:4]
    p = product(y_m).reshape(SEQS, TOK, D)
    pb[2, 2:4] = p[2:4].astype(bf16)
    send(("r", 3), pb.at[2, pl.ds(2, 2)], rb.at[1, pl.ds(2, 2)], ym)
    pf[0] = p[0:2]
    mine = product(Y).reshape(SEQS, TOK, D)
    arrived(("r", 1), rd.at[1])
    pb[1, 2:4] = (pf[1] + rd[1].astype(f32)).astype(bf16)
    send(("r", 4), pb.at[1, pl.ds(2, 2)], rb.at[0, pl.ds(2, 2)], yp)
    arrived(("r", 0), rd.at[0])
    pb[2, 0:2] = (pf[0] + rd[0].astype(f32)).astype(bf16)
    send(("r", 5), pb.at[2, pl.ds(0, 2)], rb.at[1, pl.ds(0, 2)], ym)
    arrived(("r", 2), rb.at[0, pl.ds(0, 2)])
    arrived(("r", 3), rb.at[1, pl.ds(2, 2)])
    arrived(("r", 4), rb.at[0, pl.ds(2, 2)])
    arrived(("r", 5), rb.at[1, pl.ds(0, 2)])
    out_ref[...] = (mine + rb[0].astype(f32) + rb[1].astype(f32)).astype(bf16)

    for copy in sent:
        copy.wait_send()
    for d in range(1, 8):
        k = slot("g", d)

        @pl.when(g + d < 8)
        def _():
            pltpu.make_async_remote_copy(
                src_ref=t_own,
                dst_ref=l2.at[g],
                send_sem=ssem.at[k],
                recv_sem=rsem.at[k],
                device_id=gdev(lax.rem(g + d, 8)),
                device_id_type=MESH,
            ).wait_send()


def per_device(
    tokens,
    norm_gain,
    entry_projection,
    valve_projection,
    filter_taps,
    conv_bias,
    recur_weight,
    recur_bias,
    entry_weight,
    entry_bias,
    forget_rate,
    output_weight,
):
    small = jnp.concatenate(
        [filter_taps, conv_bias[None], recur_bias[None], entry_bias[None], forget_rate[None]], axis=0
    ).reshape(8, 1, W)
    anywhere = pl.BlockSpec(memory_space=pl.ANY)
    vmem = pl.BlockSpec(memory_space=pltpu.VMEM)
    return pl.pallas_call(
        kernel,
        name="layer",
        out_shape=jax.ShapeDtypeStruct((SEQS, TOK, D), bf16),
        in_specs=[anywhere, vmem, anywhere, anywhere, anywhere, anywhere, anywhere, anywhere],
        out_specs=vmem,
        scratch_shapes=[
            pltpu.VMEM((SEQS, STR, D), bf16),
            pltpu.VMEM((ROWS, D), bf16),
            pltpu.VMEM((AROWS, CH), bf16),
            pltpu.VMEM((D, CH), bf16),
            pltpu.VMEM((CH, D), bf16),
            pltpu.VMEM((NB, 8, 1, W), f32),
            pltpu.VMEM((NB, ROWS, W), f32),
            pltpu.VMEM((NB, 32, W), f32),
            pltpu.VMEM((NB, 32, W), f32),
            pltpu.VMEM((ROWS, CH), bf16),
            pltpu.VMEM((2, ROWS, W), f32),
            pltpu.VMEM((NB, ROWS, W), f32),
            pltpu.VMEM((NB, ROWS, W), f32),
            pltpu.VMEM((NB, ROWS, W), f32),
            pltpu.VMEM((NB, ROWS, W), f32),
            pltpu.VMEM((ROWS, CH), bf16),
            pltpu.VMEM((8, CH), f32),
            pltpu.VMEM((4, 8, CH), f32),
            pltpu.VMEM((8, CH), f32),
            pltpu.VMEM((8, 8, CH), f32),
            pltpu.VMEM((3, SEQS, TOK, D), bf16),
            pltpu.VMEM((2, 2, TOK, D), f32),
            pltpu.VMEM((2, 2, TOK, D), bf16),
            pltpu.VMEM((2, SEQS, TOK, D), bf16),
            pltpu.SemaphoreType.DMA((N_COPIES,)),
            pltpu.SemaphoreType.DMA((N_COPIES,)),
            pltpu.SemaphoreType.DMA((N_LOCAL,)),
        ],
        compiler_params=pltpu.CompilerParams(
            collective_id=0, has_side_effects=True, vmem_limit_bytes=48 * 1024 * 1024
        ),
    )(
        tokens,
        norm_gain.reshape(1, D),
        entry_projection,
        valve_projection,
        recur_weight,
        entry_weight,
        small,
        output_weight,
    )


def solution(mesh):
    fine = Mesh(mesh.devices.reshape(4, 2, 4, 4), ("x", "c", "z", "y"))
    SP, TP = ("x", "c"), ("z", "y")
    both = SP + TP
    placed = (
        P(None, both, None),
        P(),
        P(None, TP),
        P(None, TP),
        P(None, TP),
        P(TP),
        P(TP, None, None),
        P(TP),
        P(TP, None, None),
        P(TP),
        P(TP),
        P(TP, None),
    )
    return jax.shard_map(
        per_device, mesh=fine, in_specs=placed, out_specs=P(None, both, None), check_vma=False
    )
```

time: 190 us -> 58 us (0.31)
  waiting for transfers between devices: 124 us -> 0 us
  Pallas kernels: 0 us -> 50.5 us
  blocking collectives: 26.7 us -> 0 us
  between operations: 13.8 us -> 0.05 us
  matrix products: 13 us -> 0 us
  other arithmetic: 4.47 us -> 0 us
  starting transfers between devices: 4.19 us -> 0 us
  local copies, waits for them, and re-layouts: 3.05 us -> 7.04 us
    reduce_scatter x2 -> x0, waiting for transfers between devices: 69.6 us -> none  [sum_by_axis(): running = lax.psum_scatter(running, axis, scatter_dimension=0, tiled=True)]
    all_gather x1 -> x0, waiting for transfers between devices: 53.5 us -> none  [over_all(): return work(lax.all_gather(shard, axis, axis=dim, tiled=True), jnp.int32(0))]
    pallas_call x0 -> x1, Pallas kernels: none -> 50.5 us  [per_device(): pl.pallas_call(kernel, name='layer', out_shape=jax.ShapeDtypeStruct((SEQS...]
    all_gather x2 -> x0, blocking collectives: 26.7 us -> none  [entering_2(): gathered = jax.tree.map(lambda a: lax.all_gather(a, axis), part)]
    dot_general x4 -> x0, matrix products: 13 us -> none  [the longest x1 8.52 us: output_term(): jnp.einsum('slc,cd->lsd', segment, output_weight, preferred_element_type=...]
    unnamed x16 -> x25, local copies, waits for them, and re-layouts: 0.04 us -> 7.02 us
    ppermute x1 -> x0, starting transfers between devices: 4.1 us -> none  [from_behind(): return lax.ppermute(value, axis, pairs)]
    convert_element_type x3 -> x0, other arithmetic: 2.12 us -> none  [the longest x1 1.81 us: per_device(): rescaled_values = (scaled * norm_gain).astype(jnp.bfloat16)]
  transfers between devices with their start and end apart: 4 -> 0, of which waited for: 4 -> 0; matrix products, arithmetic and copies ran while one was open for 0% -> 0% of each run, Pallas kernels for 0% -> 0%
where the time goes in v1:
time: 58 us; the launch traced here: 57.6 us
  Pallas kernels  50.5 us (87%)
  local copies, waits for them, and re-layouts  7.04 us (12%)
    pallas_call x1, Pallas kernels, per_device(): pl.pallas_call(kernel, name='layer', out_shape=jax.ShapeDtypeStruct((SEQS...  50.5 us
    unnamed x25, local copies, waits for them, and re-layouts  7.02 us

profile of v1, /device:TPU:1, one launch (start us, length us, event | category | flops | bytes accessed | tf_op | source)
XLA Modules:
  0.0 57.6 jit_solution(16001060662086285358)
XLA Ops:
  0.0 0.0 copy-start.7
  0.0 0.0 copy-start.8
  0.0 0.0 copy-start.9
  0.0 0.0 copy-start.10
  0.0 0.0 copy-start.11
  0.0 0.0 copy-start.6
  0.0 0.6 %copy-done.7 = f32[4,128]{1,0:T(4,128)S(1)} copy-done((f32[4,128]{1,0:T(4,128)S(1)}, f32[4,128]{1,0:T(4,128)}, u32[]{:S(2)}) %copy-start.7) | copy-done | bytes 2072
  0.7 0.0 copy-done.8
  0.7 0.0 copy-done.9
  0.7 0.0 copy-done.10
  0.7 0.0 copy-done.11
  0.7 0.0 copy-done.6
  0.8 0.0 copy-start
  0.8 1.0 %copy-done = bf16[2048,128]{1,0:T(8,128)(2,1)S(1)} copy-done((bf16[2048,128]{1,0:T(8,128)(2,1)S(1)}, bf16[2048,128]{1,0:T(8,128)(2,1)}, u32[]{:S(2)}) %copy-start) | copy-done | bytes 524312
  1.8 0.0 copy-start.1
  1.8 1.0 %copy-done.1 = bf16[2048,128]{1,0:T(8,128)(2,1)S(1)} copy-done((bf16[2048,128]{1,0:T(8,128)(2,1)S(1)}, bf16[2048,128]{1,0:T(8,128)(2,1)}, u32[]{:S(2)}) %copy-start.1) | copy-done | bytes 524312
  2.9 0.0 copy-start.2
  2.9 1.0 %copy-done.2 = bf16[128,2048]{1,0:T(8,128)(2,1)S(1)} copy-done((bf16[128,2048]{1,0:T(8,128)(2,1)S(1)}, bf16[128,2048]{1,0:T(8,128)(2,1)}, u32[]{:S(2)}) %copy-start.2) | copy-done | bytes 524312
  3.9 0.0 copy-start.3
  3.9 0.9 %copy-done.3 = bf16[4,16,2048]{2,1,0:T(8,128)(2,1)S(1)} copy-done((bf16[4,16,2048]{2,1,0:T(8,128)(2,1)S(1)}, bf16[4,16,2048]{2,1,0:T(8,128)(2,1)}, u32[]{:S(2)}) %copy-start.3) | copy-done | bytes 262168
  4.9 0.8 %copy-done.4 = bf16[1,128,128]{2,1,0:T(8,128)(2,1)S(1)} copy-done((bf16[1,128,128]{2,1,0:T(8,128)(2,1)S(1)}, bf16[1,128,128]{2,1,0:T(8,128)(2,1)}, u32[]{:S(2)}) %copy-start.4) | copy-done | bytes 32792
  5.6 0.8 %copy-done.5 = bf16[1,128,128]{2,1,0:T(8,128)(2,1)S(1)} copy-done((bf16[1,128,128]{2,1,0:T(8,128)(2,1)S(1)}, bf16[1,128,128]{2,1,0:T(8,128)(2,1)}, u32[]{:S(2)}) %copy-start.5) | copy-done | bytes 32792
  6.4 50.5 %layer.1 = bf16[4,16,2048]{2,1,0:T(8,128)(2,1)S(1)} custom-call(bf16[4,16,2048]{2,1,0:T(8,128)(2,1)S(1)} %copy-done.3, f32[1,2048]{1,0:T(1,128)S(1)} %bitcast.7, bf16[2048,128]{1,0:T(8,128)(2,1)S(1)} %copy-done, bf16[2048,128]{1,0:T(8,128)(2,1)S(1)} %copy-done.1, bf16[1,128,128]{2,1,0:T(8,128)(2,1)S(1)} %copy-done.4, bf16[1,128,128]{2,1,0:T(8,128)(2,1)S(1)} %copy-done.5, ...), custom_call_target="tpu_custom_call" | custom-call | tf_op jit(solution)/shard_map/layer/pallas_call | solution.py:490
  56.9 0.7 %copy.14 = bf16[4,16,2048]{2,1,0:T(8,128)(2,1)} copy(bf16[4,16,2048]{2,1,0:T(8,128)(2,1)S(1)} %layer.1) | data formatting | bytes 524288
  (3 shorter events, 0.0 us)
Async XLA Ops:
  0.0 0.7 %copy-start.7 = (f32[4,128]{1,0:T(4,128)S(1)}, f32[4,128]{1,0:T(4,128)}, u32[]{:S(2)}) copy-start(f32[4,128]{1,0:T(4,128)} %param.16) | copy-start | bytes 6148
  0.0 0.7 %copy-start.8 = (f32[128]{0:T(128)S(1)}, f32[128]{0:T(128)}, u32[]{:S(2)}) copy-start(f32[128]{0:T(128)} %param.17) | copy-start | bytes 1540
  0.0 0.7 %copy-start.9 = (f32[128]{0:T(128)S(1)}, f32[128]{0:T(128)}, u32[]{:S(2)}) copy-start(f32[128]{0:T(128)} %param.19) | copy-start | bytes 1540
  0.0 0.7 %copy-start.10 = (f32[128]{0:T(128)S(1)}, f32[128]{0:T(128)}, u32[]{:S(2)}) copy-start(f32[128]{0:T(128)} %param.21) | copy-start | bytes 1540
  0.0 0.7 %copy-start.11 = (f32[128]{0:T(128)S(1)}, f32[128]{0:T(128)}, u32[]{:S(2)}) copy-start(f32[128]{0:T(128)} %param.22) | copy-start | bytes 1540
  0.0 0.7 %copy-start.6 = (f32[2048]{0:T(1024)S(1)}, f32[2048]{0:T(1024)}, u32[]{:S(2)}) copy-start(f32[2048]{0:T(1024)} %param.13) | copy-start | bytes 24580
  0.8 1.0 %copy-start = (bf16[2048,128]{1,0:T(8,128)(2,1)S(1)}, bf16[2048,128]{1,0:T(8,128)(2,1)}, u32[]{:S(2)}) copy-start(bf16[2048,128]{1,0:T(8,128)(2,1)} %w1_ref.1) | copy-start | bytes 1572868
  1.8 1.0 %copy-start.1 = (bf16[2048,128]{1,0:T(8,128)(2,1)S(1)}, bf16[2048,128]{1,0:T(8,128)(2,1)}, u32[]{:S(2)}) copy-start(bf16[2048,128]{1,0:T(8,128)(2,1)} %w2_ref.1) | copy-start | bytes 1572868
  2.9 1.0 %copy-start.2 = (bf16[128,2048]{1,0:T(8,128)(2,1)S(1)}, bf16[128,2048]{1,0:T(8,128)(2,1)}, u32[]{:S(2)}) copy-start(bf16[128,2048]{1,0:T(8,128)(2,1)} %wo_ref.1) | copy-start | bytes 1572868
  3.9 0.9 %copy-start.3 = (bf16[4,16,2048]{2,1,0:T(8,128)(2,1)S(1)}, bf16[4,16,2048]{2,1,0:T(8,128)(2,1)}, u32[]{:S(2)}) copy-start(bf16[4,16,2048]{2,1,0:T(8,128)(2,1)} %tok_ref.1) | copy-start | bytes 786436
  4.9 0.8 %copy-start.4 = (bf16[1,128,128]{2,1,0:T(8,128)(2,1)S(1)}, bf16[1,128,128]{2,1,0:T(8,128)(2,1)}, u32[]{:S(2)}) copy-start(bf16[1,128,128]{2,1,0:T(8,128)(2,1)} %rw_ref.1) | copy-start | bytes 98308
  5.6 0.8 %copy-start.5 = (bf16[1,128,128]{2,1,0:T(8,128)(2,1)S(1)}, bf16[1,128,128]{2,1,0:T(8,128)(2,1)}, u32[]{:S(2)}) copy-start(bf16[1,128,128]{2,1,0:T(8,128)(2,1)} %ew_ref.1) | copy-start | bytes 98308

commit v2 on v1

--- a/solution.py
+++ b/solution.py
@@ -33,6 +33,7 @@
 
 N_COPIES = 104
 N_LOCAL = 16
+VMEM_LIMIT = 67043328
 
 
 def neg_expm1(t):
@@ -53,9 +54,14 @@
     w2_ref,
     rw_ref,
     ew_ref,
-    small_ref,
+    taps_ref,
+    cb_ref,
+    rb_ref,
+    eb_ref,
+    rate_ref,
     wo_ref,
     out_ref,
+    gain,
     tr,
     nt,
     wa,
@@ -111,6 +117,14 @@
     slot = Slots()
     local = Slots()
     sent = []
+    scopes = []
+
+    def mark(name):
+        if scopes:
+            scopes.pop().__exit__(None, None, None)
+        if name:
+            scopes.append(jax.named_scope(name))
+            scopes[-1].__enter__()
 
     def send(key, src, dst, dev):
         k = slot(*key)
@@ -141,6 +155,7 @@
         copy.start()
         return copy
 
+    mark("own")
     lanes = pl.ds(pl.multiple_of(Z * W, W), W)
     own_tok = tr.at[:, pl.ds(pl.multiple_of(Y * TOK, TOK), TOK), :]
     c_tok = fetch("tok", tok_ref, own_tok)
@@ -149,12 +164,16 @@
         fetch("rw", rw_ref.at[0], wa.at[pl.ds(D, W), lanes]),
         fetch("ew", ew_ref.at[0], wa.at[pl.ds(D + W, W), lanes]),
     ]
-    c_sm = fetch("small", small_ref, sm.at[Z])
+    c_sm = [fetch("taps", taps_ref, sm.at[Z, pl.ds(0, 4)])]
+    for n, ref in enumerate((cb_ref, rb_ref, eb_ref, rate_ref)):
+        c_sm.append(fetch(("row", n), ref, sm.at[Z, 4 + n]))
+    c_gain = fetch("gain", gain_ref, gain)
     c_wv = fetch("w2", w2_ref, wv.at[:, lanes])
     c_wo = fetch("wo", wo_ref, wog.at[pl.ds(pl.multiple_of(Z * W, W), W), :])
 
     l2[...] = jnp.zeros_like(l2)
 
+    mark("barrier")
     barrier = pltpu.get_barrier_semaphore()
     partners = [yp, ym] + [{"z": mod4(Z + d)} for d in (1, 2, 3)]
     partners += [gdev(lax.rem(g + d, 8)) for d in range(1, 8)] + [nxt, prv]
@@ -162,6 +181,7 @@
         pl.semaphore_signal(barrier, inc=1, device_id=dev, device_id_type=MESH)
     pl.semaphore_wait(barrier, len(partners))
 
+    mark("tokens")
     def tok(y, half):
         return tr.at[pl.ds(2 * half, 2), pl.ds(pl.multiple_of(y * TOK, TOK), TOK), :]
 
@@ -209,10 +229,12 @@
                     q = par if src == 0 else 1 - par
                     arrived(("d", m, j, src, h), piece(m, blocks[j], q, 1 - C, h))
 
+    mark("weights")
     for c in c_wa:
         c.wait()
     own_send(0)
-    c_sm.wait()
+    for c in c_sm:
+        c.wait()
     for d in (1, 2, 3):
         send(("s", d), sm.at[Z], sm.at[Z], {"z": mod4(Z + d)})
 
@@ -220,12 +242,15 @@
         rows = pl.ds(pl.multiple_of(y * TOK, TOK), TOK)
         v = tr[pl.ds(2 * half, 2), rows, :].astype(f32)
         v = v * lax.rsqrt(jnp.mean(v * v, axis=-1, keepdims=True) + EPS)
-        v = (v * gain_ref[...].reshape(1, 1, D)).astype(bf16)
+        v = (v * gain[...].reshape(1, 1, D)).astype(bf16)
         for s in range(2):
             nt[pl.ds(pl.multiple_of((2 * half + s) * STR + y * TOK, TOK), TOK), :] = v[s]
 
+    mark("norm0")
+    c_gain.wait()
     norm(Y, 0)
     norm(Y, 1)
+    mark("net0")
     z_event(0, 0, 0)
     z_event(0, 1, 1)
     c_wv.wait()
@@ -234,10 +259,13 @@
     send(("t", 2, 0), tok(y_m, 0), tok(y_m, 0), yp)
     arrived(("t", 1, 1), tok(y_p, 1))
     send(("t", 2, 1), tok(y_p, 1), tok(y_p, 1), ym)
+    mark("net1")
     z_event(0, 0, 1)
     z_event(0, 1, 0)
+    mark("norm1")
     norm(y_m, 0)
     norm(y_p, 1)
+    mark("net2")
     z_event(0, 2, 0)
     z_event(0, 2, 1)
     x_event(0, 0, 0)
@@ -246,26 +274,33 @@
     z_event(1, 1, 1)
     c_wo.wait()
     own_send(2)
+    mark("net3")
     x_event(0, 0, 1)
     x_event(0, 1, 0)
+    mark("norm2")
     arrived(("t", 0, 1), tok(y_m, 1))
     norm(y_m, 1)
     arrived(("t", 1, 0), tok(y_p, 0))
     norm(y_p, 0)
+    mark("net4")
     z_event(1, 0, 1)
     z_event(1, 1, 0)
     x_event(0, 2, 0)
     x_event(0, 2, 1)
+    mark("norm3")
     arrived(("t", 2, 0), tok(y_d, 0))
     norm(y_d, 0)
     arrived(("t", 2, 1), tok(y_d, 1))
     norm(y_d, 1)
+    mark("net5")
     z_event(1, 2, 0)
     z_event(1, 2, 1)
     x_event(1, 0, 0)
     x_event(1, 1, 1)
+    mark("d0")
     d_events(0)
 
+    mark("matmul1")
     conv_in = jnp.dot(nt[...], wa[0:D, :], preferred_element_type=f32).astype(bf16)
     for b in range(NB):
         part = conv_in[:, b * W : (b + 1) * W]
@@ -273,6 +308,7 @@
         for s in range(SEQS):
             hs[b, s * 8 : s * 8 + 8, :] = ci[b, s * STR + STR - 8 : s * STR + STR, :]
     send(("h",), hs, hr, nxt)
+    mark("net6")
     for d in (1, 2, 3):
         arrived(("s", d), sm.at[mod4(Z - d)])
     x_event(1, 0, 1)
@@ -281,8 +317,10 @@
     z_event(2, 1, 1)
     x_event(1, 2, 0)
     x_event(1, 2, 1)
+    mark("halo")
     arrived(("h",), hr)
 
+    mark("conv")
     lane_row = lax.broadcasted_iota(jnp.int32, (8, W), 0)
     first = jnp.where(jnp.logical_and(g == 0, Z == 0), 0.0, 1.0).astype(f32)
     for b in range(NB):
@@ -307,6 +345,7 @@
                 rows.append(acc)
             cv[pl.ds(s * STR, STR), b * W : (b + 1) * W] = jnp.concatenate(rows, axis=0).astype(bf16)
 
+    mark("gates")
     ends_a = [[None] * SEQS for _ in range(NB)]
     for b in range(NB):
         cols = slice(b * W, (b + 1) * W)
@@ -344,6 +383,7 @@
                 jnp.where(lane_row >= 1, pltpu.roll(h, 1, 0), 0.0),
             )
 
+    mark("states")
     for d in (1, 2, 3):
         send(("e", d), s_own, l1.at[Z], {"z": mod4(Z + d)})
     l1[Z] = s_own[...]
@@ -351,6 +391,7 @@
     z_event(2, 1, 0)
     x_event(2, 0, 0)
     x_event(2, 1, 1)
+    mark("states1")
     for d in (1, 2, 3):
         arrived(("e", d), l1.at[mod4(Z - d)])
     total_a, total_h = l1[0, 0:4], l1[0, 4:8]
@@ -374,15 +415,18 @@
                 device_id_type=MESH,
             ).start()
 
+    mark("net8")
     z_event(2, 2, 0)
     z_event(2, 2, 1)
     d_events(1)
     x_event(2, 0, 1)
     x_event(2, 1, 0)
+    mark("valve")
     logits = jnp.dot(nt[...], wv[...], preferred_element_type=f32).astype(bf16).astype(f32)
     for b in range(NB):
         v = logits[:, b * W : (b + 1) * W]
         sg[b] = v / (1.0 + jnp.exp(-v))
+    mark("states2")
     x_event(2, 2, 0)
     x_event(2, 2, 1)
     for d in range(1, 8):
@@ -400,12 +444,14 @@
                 device_id_type=MESH,
             ).wait_recv()
 
+    mark("entering")
     state = jnp.zeros((SEQS, CH), f32)
     for k in range(7):
         state = jnp.where(k < g, l2[k, 0:4] * state + l2[k, 4:8], state)
     for k in range(3):
         state = jnp.where(k < Z, l1[k, 0:4] * state + l1[k, 4:8], state)
 
+    mark("gated")
     for b in range(NB):
         cols = slice(b * W, (b + 1) * W)
         for s in range(SEQS):
@@ -418,6 +464,7 @@
                 gt[b, places, :] = h * sg[b, places, :]
         g16[:, cols] = gt[b].astype(bf16)
 
+    mark("d2")
     d_events(2)
 
     def product(y):
@@ -426,10 +473,12 @@
         )
         return jnp.dot(lhs, wog[...], preferred_element_type=f32)
 
+    mark("prod0")
     p = product(y_d).astype(bf16).reshape(SEQS, TOK, D)
     pb[0] = p
     send(("r", 0), pb.at[0, pl.ds(0, 2)], rd.at[0], ym)
     send(("r", 1), pb.at[0, pl.ds(2, 2)], rd.at[1], yp)
+    mark("prod1")
     p = product(y_p).reshape(SEQS, TOK, D)
     pb[1, 0:2] = p[0:2].astype(bf16)
     send(("r", 2), pb.at[1, pl.ds(0, 2)], rb.at[0, pl.ds(0, 2)], yp)
@@ -439,18 +488,22 @@
     send(("r", 3), pb.at[2, pl.ds(2, 2)], rb.at[1, pl.ds(2, 2)], ym)
     pf[0] = p[0:2]
     mine = product(Y).reshape(SEQS, TOK, D)
+    mark("red1")
     arrived(("r", 1), rd.at[1])
     pb[1, 2:4] = (pf[1] + rd[1].astype(f32)).astype(bf16)
     send(("r", 4), pb.at[1, pl.ds(2, 2)], rb.at[0, pl.ds(2, 2)], yp)
     arrived(("r", 0), rd.at[0])
     pb[2, 0:2] = (pf[0] + rd[0].astype(f32)).astype(bf16)
     send(("r", 5), pb.at[2, pl.ds(0, 2)], rb.at[1, pl.ds(0, 2)], ym)
+    mark("red2")
     arrived(("r", 2), rb.at[0, pl.ds(0, 2)])
     arrived(("r", 3), rb.at[1, pl.ds(2, 2)])
     arrived(("r", 4), rb.at[0, pl.ds(2, 2)])
     arrived(("r", 5), rb.at[1, pl.ds(0, 2)])
+    mark("final")
     out_ref[...] = (mine + rb[0].astype(f32) + rb[1].astype(f32)).astype(bf16)
 
+    mark("drain")
     for copy in sent:
         copy.wait_send()
     for d in range(1, 8):
@@ -466,6 +519,8 @@
                 device_id=gdev(lax.rem(g + d, 8)),
                 device_id_type=MESH,
             ).wait_send()
+
+    mark(None)
 
 
 def per_device(
@@ -482,18 +537,16 @@
     forget_rate,
     output_weight,
 ):
-    small = jnp.concatenate(
-        [filter_taps, conv_bias[None], recur_bias[None], entry_bias[None], forget_rate[None]], axis=0
-    ).reshape(8, 1, W)
-    anywhere = pl.BlockSpec(memory_space=pl.ANY)
+    hbm = pl.BlockSpec(memory_space=pltpu.HBM)
     vmem = pl.BlockSpec(memory_space=pltpu.VMEM)
     return pl.pallas_call(
         kernel,
         name="layer",
         out_shape=jax.ShapeDtypeStruct((SEQS, TOK, D), bf16),
-        in_specs=[anywhere, vmem, anywhere, anywhere, anywhere, anywhere, anywhere, anywhere],
+        in_specs=[hbm] * 12,
         out_specs=vmem,
         scratch_shapes=[
+            pltpu.VMEM((1, D), f32),
             pltpu.VMEM((SEQS, STR, D), bf16),
             pltpu.VMEM((ROWS, D), bf16),
             pltpu.VMEM((AROWS, CH), bf16),
@@ -523,7 +576,7 @@
             pltpu.SemaphoreType.DMA((N_LOCAL,)),
         ],
         compiler_params=pltpu.CompilerParams(
-            collective_id=0, has_side_effects=True, vmem_limit_bytes=48 * 1024 * 1024
+            collective_id=0, has_side_effects=True, vmem_limit_bytes=VMEM_LIMIT
         ),
     )(
         tokens,
@@ -532,7 +585,11 @@
         valve_projection,
         recur_weight,
         entry_weight,
-        small,
+        filter_taps.reshape(4, 1, W),
+        conv_bias.reshape(1, W),
+        recur_bias.reshape(1, W),
+        entry_bias.reshape(1, W),
+        forget_rate.reshape(1, W),
         output_weight,
     )
 

time: 58 us -> 52.8 us (0.910)
  local copies, waits for them, and re-layouts: 7.04 us -> 1.67 us
    unnamed x25 -> x1, local copies, waits for them, and re-layouts: 7.02 us -> 1.67 us
where the time goes in v2:
time: 52.8 us; the launch traced here: 52.7 us
  Pallas kernels  51 us (97%)
  local copies, waits for them, and re-layouts  1.67 us (3%)
    pallas_call x1, Pallas kernels, per_device(): pl.pallas_call(kernel, name='layer', out_shape=jax.ShapeDtypeStruct((SEQS...  51 us
    unnamed x1, local copies, waits for them, and re-layouts  1.67 us

profile of v2, /device:TPU:1, one launch (start us, length us, event | category | flops | bytes accessed | tf_op | source)
XLA Modules:
  0.0 52.7 jit_solution(9470141127134849333)
XLA Ops:
  0.0 51.0 %layer.1 = bf16[4,16,2048]{2,1,0:T(8,128)(2,1)} custom-call(bf16[4,16,2048]{2,1,0:T(8,128)(2,1)} %tok_ref.1, f32[1,2048]{1,0:T(1,128)} %bitcast.6, bf16[2048,128]{1,0:T(8,128)(2,1)} %w1_ref.1, bf16[2048,128]{1,0:T(8,128)(2,1)} %w2_ref.1, bf16[1,128,128]{2,1,0:T(8,128)(2,1)} %rw_ref.1, bf16[1,128,128]{2,1,0:T(8,128)(2,1)} %ew_ref.1, f32[4,1,128]{2,1,0:T(1,128)} %bitcast.7, ...), custom_call_target="tpu_custom_call" | custom-call | tf_op jit(solution)/shard_map/layer/pallas_call | solution.py:542
  51.0 1.7 %copy.14 = bf16[4,16,2048]{2,1,0:T(8,128)(2,1)} copy(bf16[4,16,2048]{2,1,0:T(8,128)(2,1)} %layer.1) | data formatting | bytes 524288

commit v3 on v2

v3 whole, which is shorter than its diff:
```python
import jax
import jax.numpy as jnp
from jax import lax
from jax.experimental import pallas as pl
from jax.experimental.pallas import tpu as pltpu
from jax.sharding import Mesh
from jax.sharding import PartitionSpec as P

MESH = pl.DeviceIdType.MESH
EPS = 1e-06
POWER = 8.0
SEQS = 4
TOK = 16
STR = 64
D = 2048
W = 128
NB = 4
CH = NB * W
ROWS = SEQS * STR
AROWS = D + 2 * W
PIECE = ((AROWS // 16, 0), (AROWS // 16, AROWS // 2), (D // 8, 0), (W // 8, 0))
f32 = jnp.float32
bf16 = jnp.bfloat16


class Slots:
    def __init__(self):
        self.index = {}

    def __call__(self, *key):
        return self.index.setdefault(key, len(self.index))


N_COPIES = 74
N_SENDS = 16
N_LOCAL = 7
VMEM_LIMIT = 67043328


def neg_expm1(t):
    s = 1.0 + t * (1.0 / 8.0)
    for n in (7.0, 6.0, 5.0, 4.0, 3.0, 2.0):
        s = 1.0 + t * (1.0 / n) * s
    return jnp.where(t > -0.5, -t * s, 1.0 - jnp.exp(t))


def sigmoid(v):
    return 1.0 / (1.0 + jnp.exp(-v))


def kernel(
    tok_ref,
    gain_ref,
    w1_ref,
    w2_ref,
    rw_ref,
    ew_ref,
    taps_ref,
    cb_ref,
    rb_ref,
    eb_ref,
    rate_ref,
    wo_ref,
    out_ref,
    gain,
    tr,
    nt,
    wa,
    wv,
    wog,
    sm,
    ci,
    hs,
    hr,
    cv,
    lg,
    de,
    pu,
    sg,
    gt,
    g16,
    s_own,
    l1,
    t_own,
    l2,
    pb,
    pf,
    rd,
    rb,
    ob,
    ssem,
    rsem,
    lsem,
):
    X = lax.axis_index("x")
    C = lax.axis_index("c")
    Z = lax.axis_index("z")
    Y = lax.axis_index("y")
    g = X * 2 + C
    par = lax.rem(X, 2)

    def mod4(v):
        return lax.rem(v + 8, 4)

    def gdev(v):
        return {"x": v // 2, "c": lax.rem(v, 2)}

    nxt_z = mod4(Z + 1)
    nxt_g = lax.rem(g + jnp.where(Z == 3, 1, 0), 8)
    prv_z = mod4(Z - 1)
    prv_g = lax.rem(g + 8 - jnp.where(Z == 0, 1, 0), 8)
    nxt = {"x": nxt_g // 2, "c": lax.rem(nxt_g, 2), "z": nxt_z}
    prv = {"x": prv_g // 2, "c": lax.rem(prv_g, 2), "z": prv_z}
    yp, ym = {"y": mod4(Y + 1)}, {"y": mod4(Y - 1)}
    zp, zm = {"z": nxt_z}, {"z": prv_z}
    xp, xm = {"x": mod4(X + 1)}, {"x": mod4(X - 1)}
    mate = {"c": 1 - C}

    slot = Slots()
    local = Slots()
    scopes = []

    def mark(name):
        if scopes:
            scopes.pop().__exit__(None, None, None)
        if name:
            scopes.append(jax.named_scope(name))
            scopes[-1].__enter__()

    def remote(out, key, src, dst, dev):
        return pltpu.make_async_remote_copy(
            src_ref=src,
            dst_ref=dst,
            send_sem=ssem.at[out],
            recv_sem=rsem.at[slot(*key)],
            device_id=dev,
            device_id_type=MESH,
        )

    def send(out, key, src, dst, dev):
        remote(out, key, src, dst, dev).start()

    def arrived(key, dst):
        remote(0, key, dst, dst, mate).wait_recv()

    def left(out, ref):
        remote(out, ("t", 0, 0), ref, ref, mate).wait_send()

    def fetch(key, src, dst):
        copy = pltpu.make_async_copy(src, dst, lsem.at[local(key)])
        copy.start()
        return copy

    mark("own")
    own_tok = tr.at[:, pl.ds(pl.multiple_of(Y * TOK, TOK), TOK), :]
    c_tok = fetch("tok", tok_ref, own_tok)
    fetch("wa", w1_ref, wa.at[Z, pl.ds(0, D)])
    fetch("wa", rw_ref.at[0], wa.at[Z, pl.ds(D, W)])
    fetch("wa", ew_ref.at[0], wa.at[Z, pl.ds(D + W, W)])
    fetch("sm", taps_ref, sm.at[Z, pl.ds(0, 4)])
    for n, ref in enumerate((cb_ref, rb_ref, eb_ref, rate_ref)):
        fetch("sm", ref, sm.at[Z, 4 + n])
    c_gain = fetch("gain", gain_ref, gain)
    c_wv = fetch("w2", w2_ref, wv.at[Z])
    c_wo = fetch("wo", wo_ref, wog.at[Z])

    l2[...] = jnp.zeros_like(l2)

    mark("barrier")
    barrier = pltpu.get_barrier_semaphore()
    partners = [yp, ym] + [{"z": mod4(Z + d)} for d in (1, 2, 3)]
    partners += [gdev(lax.rem(g + d, 8)) for d in range(1, 8)] + [nxt, prv]
    for dev in partners:
        pl.semaphore_signal(barrier, inc=1, device_id=dev, device_id_type=MESH)
    pl.semaphore_wait(barrier, len(partners))

    mark("tokens")
    def tok(y, half):
        return tr.at[pl.ds(2 * half, 2), pl.ds(pl.multiple_of(y * TOK, TOK), TOK), :]

    y_m, y_p, y_d = mod4(Y - 1), mod4(Y + 1), mod4(Y + 2)
    c_tok.wait()
    send(0, ("t", 0, 0), tok(Y, 0), tok(Y, 0), yp)
    send(0, ("t", 1, 1), tok(Y, 1), tok(Y, 1), ym)
    send(0, ("t", 0, 1), tok(Y, 1), tok(Y, 1), yp)
    send(0, ("t", 1, 0), tok(Y, 0), tok(Y, 0), ym)

    def piece(m, z, q, core, h):
        rows, base = PIECE[m]
        k = q * 4 + core * 2 + h
        place = pl.ds(pl.multiple_of(base + k * rows, 16), rows)
        if m == 3:
            return wog.at[z, place]
        return (wa, wa, wv)[m].at[z, place]

    blocks = (mod4(Z - 1), mod4(Z + 1), mod4(Z + 2))

    def own_send(m):
        for j, h, dev in ((0, 0, zp), (1, 1, zm), (0, 1, zp), (1, 0, zm)):
            ref = piece(m, Z, par, C, h)
            send(1 + m, ("z", m, j, h), ref, ref, dev)

    def z_event(m, j, h):
        ref = piece(m, blocks[j], par, C, h)
        arrived(("z", m, j, h), ref)
        if (j, h) == (0, 0):
            send(1 + m, ("z", m, 2, 0), ref, ref, zp)
        if (j, h) == (1, 1):
            send(1 + m, ("z", m, 2, 1), ref, ref, zm)
        send(1 + m, ("x", m, j, h), ref, ref, xp if h == 0 else xm)
        send(1 + m, ("d", m), ref, ref, mate)

    def x_event(m, j, h):
        ref = piece(m, blocks[j], 1 - par, C, h)
        arrived(("x", m, j, h), ref)
        send(1 + m, ("d", m), ref, ref, mate)

    def near_z(m):
        z_event(m, 0, 0)
        z_event(m, 1, 1)

    def next_z(m):
        z_event(m, 0, 1)
        z_event(m, 1, 0)

    def far_z(m):
        z_event(m, 2, 0)
        z_event(m, 2, 1)

    def near_x(m):
        x_event(m, 0, 0)
        x_event(m, 1, 1)

    def next_x(m):
        x_event(m, 0, 1)
        x_event(m, 1, 0)

    def far_x(m):
        x_event(m, 2, 0)
        x_event(m, 2, 1)

    def volume(m, parts):
        return (wa, wa, wv, wog)[m].at[pl.ds(0, parts // 6), pl.ds(0, PIECE[m][0] * 6)]

    mark("weights")
    pltpu.make_async_copy(wa.at[0], wa.at[0], lsem.at[local("wa")]).wait()
    own_send(0)
    own_send(1)
    pltpu.make_async_copy(sm.at[0], sm.at[0], lsem.at[local("sm")]).wait()
    for d in (1, 2, 3):
        send(5, ("s",), sm.at[Z], sm.at[Z], {"z": mod4(Z + d)})

    def norm(y, half):
        rows = pl.ds(pl.multiple_of(y * TOK, TOK), TOK)
        v = tr[pl.ds(2 * half, 2), rows, :].astype(f32)
        v = v * lax.rsqrt(jnp.mean(v * v, axis=-1, keepdims=True) + EPS)
        v = (v * gain[...].reshape(1, 1, D)).astype(bf16)
        for s in range(2):
            nt[pl.ds(pl.multiple_of((2 * half + s) * STR + y * TOK, TOK), TOK), :] = v[s]

    mark("norm0")
    c_gain.wait()
    norm(Y, 0)
    norm(Y, 1)
    mark("net0")
    near_z(0)
    near_z(1)
    c_wv.wait()
    own_send(2)
    mark("net1")
    arrived(("t", 0, 0), tok(y_m, 0))
    send(0, ("t", 2, 0), tok(y_m, 0), tok(y_m, 0), yp)
    arrived(("t", 1, 1), tok(y_p, 1))
    send(0, ("t", 2, 1), tok(y_p, 1), tok(y_p, 1), ym)
    mark("net2")
    next_z(0)
    next_z(1)
    mark("norm1")
    norm(y_m, 0)
    norm(y_p, 1)
    mark("net3")
    near_x(0)
    near_x(1)
    far_z(0)
    far_z(1)
    next_x(0)
    next_x(1)
    mark("net3t")
    arrived(("t", 0, 1), tok(y_m, 1))
    arrived(("t", 1, 0), tok(y_p, 0))
    mark("norm2")
    norm(y_m, 1)
    norm(y_p, 0)
    mark("net4")
    near_z(2)
    c_wo.wait()
    own_send(3)
    mark("net5")
    far_x(0)
    far_x(1)
    mark("net5t")
    arrived(("t", 2, 0), tok(y_d, 0))
    norm(y_d, 0)
    arrived(("t", 2, 1), tok(y_d, 1))
    norm(y_d, 1)
    mark("d0")
    arrived(("d", 0), volume(0, 12))
    arrived(("d", 1), volume(1, 12))

    mark("matmul1")

    def pair(ref, b):
        rhs = jnp.concatenate([ref[b, 0:D, :], ref[b + 1, 0:D, :]], axis=1)
        return jnp.dot(nt[...], rhs, preferred_element_type=f32).astype(bf16).astype(f32)

    for b in range(0, NB, 2):
        part = pair(wa, b)
        ci[b] = part[:, 0:W]
        ci[b + 1] = part[:, W : 2 * W]
        for n in (b, b + 1):
            for s in range(SEQS):
                last = part[s * STR + STR - 8 : s * STR + STR, (n - b) * W : (n - b + 1) * W]
                hs[n, s * 8 : s * 8 + 8, :] = last
    send(6, ("h",), hs, hr, nxt)
    mark("net6")
    next_z(2)
    arrived(("s",), sm.at[pl.ds(0, 3)])

    mark("conv")
    lane_row = lax.broadcasted_iota(jnp.int32, (8, W), 0)

    def convolve(b, at):
        acc = jnp.broadcast_to(sm[b, 4], (8, W))
        for k in range(4):
            acc = acc + at(k - 3) * sm[b, k]
        return acc

    for b in range(NB):
        for s in range(SEQS):
            x = [ci[b, pl.ds(s * STR + i, 8, stride=8), :] for i in range(8)]
            prev = {i - 8: pltpu.roll(x[i], 1, 0) for i in (5, 6, 7)}
            rows = []
            for i in range(8):
                rows.append(convolve(b, lambda n: x[i + n] if i + n >= 0 else prev[i + n]))
            cv[pl.ds(s * STR, STR), b * W : (b + 1) * W] = jnp.concatenate(rows, axis=0).astype(bf16)

    mark("gates")

    def gates(b, logit_r, logit_e, conv):
        r_gate = sigmoid(logit_r + sm[b, 5])
        e_gate = sigmoid(logit_e + sm[b, 6])
        log_decay = (-POWER * r_gate) * sm[b, 7]
        push = jnp.sqrt(neg_expm1(2.0 * log_decay)) * (e_gate * conv.astype(f32))
        return jnp.exp(log_decay), push

    def gate_dots(b, conv):
        return [
            jnp.dot(conv, wa[b, D + n * W : D + (n + 1) * W, :], preferred_element_type=f32)
            for n in range(2)
        ]

    for b in range(NB):
        cols = slice(b * W, (b + 1) * W)
        lg[0], lg[1] = gate_dots(b, cv[:, cols])
        for s in range(SEQS):
            rows = slice(s * STR, (s + 1) * STR)
            de[b, rows, :], pu[b, rows, :] = gates(b, lg[0, rows, :], lg[1, rows, :], cv[rows, cols])

    mark("net7")
    far_z(2)
    near_x(2)
    near_z(3)
    mark("halo")
    arrived(("h",), hr)
    mark("redo")
    start = jnp.logical_and(g == 0, Z == 0)
    for b in range(NB):
        tiles = []
        for s in range(SEQS):
            behind = jnp.where(start, 0.0, hr[b, s * 8 : s * 8 + 8, :])
            here = ci[b, s * STR : s * STR + 8, :]

            def at(n):
                if n == 0:
                    return here
                return jnp.where(lane_row < -n, pltpu.roll(behind, -n, 0), pltpu.roll(here, -n, 0))

            tiles.append(convolve(b, at))
        conv = jnp.concatenate(tiles, axis=0).astype(bf16)
        decay, push = gates(b, *gate_dots(b, conv), conv)
        for s in range(SEQS):
            chain = pl.ds(s * STR, 8, stride=8)
            de[b, chain, :] = decay[s * 8 : s * 8 + 8]
            pu[b, chain, :] = push[s * 8 : s * 8 + 8]

    mark("scan")
    ends = [[None] * SEQS for _ in range(NB)]
    for b in range(NB):
        cols = slice(b * W, (b + 1) * W)
        tot_a, tot_h = [], []
        for s in range(SEQS):
            a = de[b, s * STR : s * STR + 8, :]
            h = pu[b, s * STR : s * STR + 8, :]
            for i in range(1, 8):
                at = slice(s * STR + i * 8, s * STR + i * 8 + 8)
                step = de[b, at, :]
                h = step * h + pu[b, at, :]
                a = step * a
                de[b, at, :] = a
                pu[b, at, :] = h
            for n in (1, 2, 4):
                keep = lane_row >= n
                a_in = jnp.where(keep, pltpu.roll(a, n, 0), 1.0)
                h_in = jnp.where(keep, pltpu.roll(h, n, 0), 0.0)
                h = a * h_in + h
                a = a * a_in
            tot_a.append(a[7:8])
            tot_h.append(h[7:8])
            ends[b][s] = (
                jnp.where(lane_row >= 1, pltpu.roll(a, 1, 0), 1.0),
                jnp.where(lane_row >= 1, pltpu.roll(h, 1, 0), 0.0),
            )
        s_own[:, cols] = jnp.concatenate(tot_a + tot_h, axis=0).astype(bf16)

    mark("states")
    for d in (1, 2, 3):
        send(7, ("e",), s_own, l1.at[Z], {"z": mod4(Z + d)})
    l1[Z] = s_own[...]
    next_x(2)
    far_x(2)
    next_z(3)
    mark("states1")
    arrived(("e",), l1.at[pl.ds(0, 3)])
    total_a, total_h = l1[0, 0:4].astype(f32), l1[0, 4:8].astype(f32)
    for k in range(1, 4):
        ka, kh = l1[k, 0:4].astype(f32), l1[k, 4:8].astype(f32)
        total_h = ka * total_h + kh
        total_a = ka * total_a
    t_own[...] = jnp.concatenate([total_a, total_h], axis=0).astype(bf16)

    def to_group(d):
        return remote(8 + d, ("g", d), t_own, l2.at[g], gdev(lax.rem(g + d, 8)))

    for d in range(1, 8):

        @pl.when(g + d < 8)
        def _():
            to_group(d).start()

    mark("net8")
    far_z(3)
    near_x(3)
    next_x(3)
    arrived(("d", 2), volume(2, 12))
    mark("valve")
    for b in range(0, NB, 2):
        v = pair(wv, b)
        v = v / (1.0 + jnp.exp(-v))
        sg[b] = v[:, 0:W]
        sg[b + 1] = v[:, W : 2 * W]
    far_x(3)
    mark("states2")
    for d in range(1, 8):

        @pl.when(g - d >= 0)
        def _():
            arrived(("g", d), l2.at[lax.rem(g - d + 8, 8)])

    mark("entering")
    state = jnp.zeros((SEQS, CH), f32)
    for k in range(7):
        state = jnp.where(k < g, l2[k, 0:4].astype(f32) * state + l2[k, 4:8].astype(f32), state)
    for k in range(3):
        state = jnp.where(k < Z, l1[k, 0:4].astype(f32) * state + l1[k, 4:8].astype(f32), state)

    mark("gated")
    for b in range(NB):
        cols = slice(b * W, (b + 1) * W)
        for s in range(SEQS):
            chain_a, chain_h = ends[b][s]
            enter = chain_a * jnp.broadcast_to(state[s : s + 1, cols], (8, W)) + chain_h
            for i in range(8):
                at = s * STR + i * 8
                h = de[b, at : at + 8, :] * enter + pu[b, at : at + 8, :]
                places = pl.ds(s * STR + i, 8, stride=8)
                gt[b, places, :] = h * sg[b, places, :]
        g16[:, cols] = gt[b].astype(bf16)

    mark("d2")
    arrived(("d", 3), volume(3, 12))

    def product(y):
        lhs = jnp.concatenate(
            [g16[pl.ds(pl.multiple_of(s * STR + y * TOK, TOK), TOK), :] for s in range(SEQS)], axis=0
        )
        return jnp.dot(lhs, wog[...].reshape(CH, D), preferred_element_type=f32)

    mark("prod0")
    p = product(y_d).astype(bf16).reshape(SEQS, TOK, D)
    pb[0] = p
    send(8, ("r", 0), pb.at[0, pl.ds(0, 2)], rd.at[0], ym)
    send(8, ("r", 1), pb.at[0, pl.ds(2, 2)], rd.at[1], yp)
    mark("prod1")
    p = product(y_p).reshape(SEQS, TOK, D)
    pb[1, 0:2] = p[0:2].astype(bf16)
    send(8, ("r", 2), pb.at[1, pl.ds(0, 2)], rb.at[0, pl.ds(0, 2)], yp)
    pf[1] = p[2:4]
    p = product(y_m).reshape(SEQS, TOK, D)
    pb[2, 2:4] = p[2:4].astype(bf16)
    send(8, ("r", 3), pb.at[2, pl.ds(2, 2)], rb.at[1, pl.ds(2, 2)], ym)
    pf[0] = p[0:2]
    mine = product(Y).reshape(SEQS, TOK, D)
    mark("red1")
    arrived(("r", 1), rd.at[1])
    pb[1, 2:4] = (pf[1] + rd[1].astype(f32)).astype(bf16)
    send(8, ("r", 4), pb.at[1, pl.ds(2, 2)], rb.at[0, pl.ds(2, 2)], yp)
    arrived(("r", 0), rd.at[0])
    pb[2, 0:2] = (pf[0] + rd[0].astype(f32)).astype(bf16)
    send(8, ("r", 5), pb.at[2, pl.ds(0, 2)], rb.at[1, pl.ds(0, 2)], ym)
    mark("red2")
    arrived(("r", 2), rb.at[0, pl.ds(0, 2)])
    arrived(("r", 3), rb.at[1, pl.ds(2, 2)])
    arrived(("r", 4), rb.at[0, pl.ds(2, 2)])
    arrived(("r", 5), rb.at[1, pl.ds(0, 2)])
    mark("final")
    ob[...] = (mine + rb[0].astype(f32) + rb[1].astype(f32)).astype(bf16)
    c_out = fetch("out", ob, out_ref)

    mark("drain")
    left(0, tr.at[pl.ds(0, 3)])
    for m in range(4):
        left(1 + m, volume(m, 24))
    left(5, sm.at[pl.ds(0, 3)])
    left(6, hs)
    left(7, l1.at[pl.ds(0, 3)])
    left(8, pb)
    for d in range(1, 8):

        @pl.when(g + d < 8)
        def _():
            to_group(d).wait_send()

    mark("outwait")
    c_out.wait()
    assert len(slot.index) <= N_COPIES and len(local.index) <= N_LOCAL
    mark(None)


def per_device(
    tokens,
    norm_gain,
    entry_projection,
    valve_projection,
    filter_taps,
    conv_bias,
    recur_weight,
    recur_bias,
    entry_weight,
    entry_bias,
    forget_rate,
    output_weight,
):
    hbm = pl.BlockSpec(memory_space=pltpu.HBM)
    return pl.pallas_call(
        kernel,
        name="layer",
        out_shape=jax.ShapeDtypeStruct((SEQS, TOK, D), bf16),
        in_specs=[hbm] * 12,
        out_specs=hbm,
        scratch_shapes=[
            pltpu.VMEM((1, D), f32),
            pltpu.VMEM((SEQS, STR, D), bf16),
            pltpu.VMEM((ROWS, D), bf16),
            pltpu.VMEM((NB, AROWS, W), bf16),
            pltpu.VMEM((NB, D, W), bf16),
            pltpu.VMEM((NB, W, D), bf16),
            pltpu.VMEM((NB, 8, 1, W), f32),
            pltpu.VMEM((NB, ROWS, W), f32),
            pltpu.VMEM((NB, 32, W), f32),
            pltpu.VMEM((NB, 32, W), f32),
            pltpu.VMEM((ROWS, CH), bf16),
            pltpu.VMEM((2, ROWS, W), f32),
            pltpu.VMEM((NB, ROWS, W), f32),
            pltpu.VMEM((NB, ROWS, W), f32),
            pltpu.VMEM((NB, ROWS, W), f32),
            pltpu.VMEM((NB, ROWS, W), f32),
            pltpu.VMEM((ROWS, CH), bf16),
            pltpu.VMEM((8, CH), bf16),
            pltpu.VMEM((4, 8, CH), bf16),
            pltpu.VMEM((8, CH), bf16),
            pltpu.VMEM((8, 8, CH), bf16),
            pltpu.VMEM((3, SEQS, TOK, D), bf16),
            pltpu.VMEM((2, 2, TOK, D), f32),
            pltpu.VMEM((2, 2, TOK, D), bf16),
            pltpu.VMEM((2, SEQS, TOK, D), bf16),
            pltpu.VMEM((SEQS, TOK, D), bf16),
            pltpu.SemaphoreType.DMA((N_SENDS,)),
            pltpu.SemaphoreType.DMA((N_COPIES,)),
            pltpu.SemaphoreType.DMA((N_LOCAL,)),
        ],
        compiler_params=pltpu.CompilerParams(
            collective_id=0, has_side_effects=True, vmem_limit_bytes=VMEM_LIMIT
        ),
    )(
        tokens,
        norm_gain.reshape(1, D),
        entry_projection,
        valve_projection,
        recur_weight,
        entry_weight,
        filter_taps.reshape(4, 1, W),
        conv_bias.reshape(1, W),
        recur_bias.reshape(1, W),
        entry_bias.reshape(1, W),
        forget_rate.reshape(1, W),
        output_weight,
    )


def solution(mesh):
    fine = Mesh(mesh.devices.reshape(4, 2, 4, 4), ("x", "c", "z", "y"))
    SP, TP = ("x", "c"), ("z", "y")
    both = SP + TP
    placed = (
        P(None, both, None),
        P(),
        P(None, TP),
        P(None, TP),
        P(None, TP),
        P(TP),
        P(TP, None, None),
        P(TP),
        P(TP, None, None),
        P(TP),
        P(TP),
        P(TP, None),
    )
    return jax.shard_map(
        per_device, mesh=fine, in_specs=placed, out_specs=P(None, both, None), check_vma=False
    )
```

time: 52.8 us -> 49.7 us (0.941)
  Pallas kernels: 51 us -> 47.9 us
    pallas_call x1, Pallas kernels: 51 us -> 47.9 us  [per_device(): pl.pallas_call(kernel, name='layer', out_shape=jax.ShapeDtypeStruct((SEQS...]
where the time goes in v3:
time: 49.7 us; the launch traced here: 49.5 us
  Pallas kernels  47.9 us (96%)
  local copies, waits for them, and re-layouts  1.67 us (3%)
    pallas_call x1, Pallas kernels, per_device(): pl.pallas_call(kernel, name='layer', out_shape=jax.ShapeDtypeStruct((SEQS...  47.9 us
    unnamed x1, local copies, waits for them, and re-layouts  1.67 us

profile of v3, /device:TPU:1, one launch (start us, length us, event | category | flops | bytes accessed | tf_op | source)
XLA Modules:
  0.0 49.5 jit_solution(1986229469999510380)
XLA Ops:
  0.0 47.9 %layer.1 = bf16[4,16,2048]{2,1,0:T(8,128)(2,1)} custom-call(bf16[4,16,2048]{2,1,0:T(8,128)(2,1)} %tok_ref.1, f32[1,2048]{1,0:T(1,128)} %bitcast.6, bf16[2048,128]{1,0:T(8,128)(2,1)} %w1_ref.1, bf16[2048,128]{1,0:T(8,128)(2,1)} %w2_ref.1, bf16[1,128,128]{2,1,0:T(8,128)(2,1)} %rw_ref.1, bf16[1,128,128]{2,1,0:T(8,128)(2,1)} %ew_ref.1, f32[4,1,128]{2,1,0:T(1,128)} %bitcast.7, ...), custom_call_target="tpu_custom_call" | custom-call | tf_op jit(solution)/shard_map/layer/pallas_call | solution.py:564
  47.9 1.7 %copy.14 = bf16[4,16,2048]{2,1,0:T(8,128)(2,1)} copy(bf16[4,16,2048]{2,1,0:T(8,128)(2,1)} %layer.1) | data formatting | bytes 524288

commit v4 on v3

--- a/solution.py
+++ b/solution.py
@@ -9,6 +9,7 @@
 MESH = pl.DeviceIdType.MESH
 EPS = 1e-06
 POWER = 8.0
+TINY = 1e-37
 SEQS = 4
 TOK = 16
 STR = 64
@@ -34,7 +35,7 @@
 N_COPIES = 74
 N_SENDS = 16
 N_LOCAL = 7
-VMEM_LIMIT = 67043328
+VMEM_LIMIT = 66700000
 
 
 def neg_expm1(t):
@@ -87,7 +88,6 @@
     pf,
     rd,
     rb,
-    ob,
     ssem,
     rsem,
     lsem,
@@ -267,6 +267,8 @@
     near_z(1)
     c_wv.wait()
     own_send(2)
+    c_wo.wait()
+    own_send(3)
     mark("net1")
     arrived(("t", 0, 0), tok(y_m, 0))
     send(0, ("t", 2, 0), tok(y_m, 0), tok(y_m, 0), yp)
@@ -293,8 +295,6 @@
     norm(y_p, 0)
     mark("net4")
     near_z(2)
-    c_wo.wait()
-    own_send(3)
     mark("net5")
     far_x(0)
     far_x(1)
@@ -320,10 +320,12 @@
         for n in (b, b + 1):
             for s in range(SEQS):
                 last = part[s * STR + STR - 8 : s * STR + STR, (n - b) * W : (n - b + 1) * W]
-                hs[n, s * 8 : s * 8 + 8, :] = last
+                hs[n, s * 8 : s * 8 + 8, :] = last.astype(bf16)
     send(6, ("h",), hs, hr, nxt)
     mark("net6")
     next_z(2)
+    near_z(3)
+    near_x(2)
     arrived(("s",), sm.at[pl.ds(0, 3)])
 
     mark("conv")
@@ -367,9 +369,10 @@
             de[b, rows, :], pu[b, rows, :] = gates(b, lg[0, rows, :], lg[1, rows, :], cv[rows, cols])
 
     mark("net7")
+    next_z(3)
+    next_x(2)
     far_z(2)
-    near_x(2)
-    near_z(3)
+    near_x(3)
     mark("halo")
     arrived(("h",), hr)
     mark("redo")
@@ -377,7 +380,7 @@
     for b in range(NB):
         tiles = []
         for s in range(SEQS):
-            behind = jnp.where(start, 0.0, hr[b, s * 8 : s * 8 + 8, :])
+            behind = jnp.where(start, 0.0, hr[b, s * 8 : s * 8 + 8, :].astype(f32))
             here = ci[b, s * STR : s * STR + 8, :]
 
             def at(n):
@@ -420,22 +423,23 @@
                 jnp.where(lane_row >= 1, pltpu.roll(a, 1, 0), 1.0),
                 jnp.where(lane_row >= 1, pltpu.roll(h, 1, 0), 0.0),
             )
+        tot_a = [jnp.log(jnp.maximum(a, TINY)) for a in tot_a]
         s_own[:, cols] = jnp.concatenate(tot_a + tot_h, axis=0).astype(bf16)
 
     mark("states")
     for d in (1, 2, 3):
         send(7, ("e",), s_own, l1.at[Z], {"z": mod4(Z + d)})
     l1[Z] = s_own[...]
-    next_x(2)
+    far_z(3)
+    next_x(3)
     far_x(2)
-    next_z(3)
     mark("states1")
     arrived(("e",), l1.at[pl.ds(0, 3)])
     total_a, total_h = l1[0, 0:4].astype(f32), l1[0, 4:8].astype(f32)
     for k in range(1, 4):
         ka, kh = l1[k, 0:4].astype(f32), l1[k, 4:8].astype(f32)
-        total_h = ka * total_h + kh
-        total_a = ka * total_a
+        total_h = jnp.exp(ka) * total_h + kh
+        total_a = ka + total_a
     t_own[...] = jnp.concatenate([total_a, total_h], axis=0).astype(bf16)
 
     def to_group(d):
@@ -448,9 +452,7 @@
             to_group(d).start()
 
     mark("net8")
-    far_z(3)
-    near_x(3)
-    next_x(3)
+    far_x(3)
     arrived(("d", 2), volume(2, 12))
     mark("valve")
     for b in range(0, NB, 2):
@@ -458,7 +460,6 @@
         v = v / (1.0 + jnp.exp(-v))
         sg[b] = v[:, 0:W]
         sg[b + 1] = v[:, W : 2 * W]
-    far_x(3)
     mark("states2")
     for d in range(1, 8):
 
@@ -469,9 +470,9 @@
     mark("entering")
     state = jnp.zeros((SEQS, CH), f32)
     for k in range(7):
-        state = jnp.where(k < g, l2[k, 0:4].astype(f32) * state + l2[k, 4:8].astype(f32), state)
+        state = jnp.where(k < g, jnp.exp(l2[k, 0:4].astype(f32)) * state + l2[k, 4:8].astype(f32), state)
     for k in range(3):
-        state = jnp.where(k < Z, l1[k, 0:4].astype(f32) * state + l1[k, 4:8].astype(f32), state)
+        state = jnp.where(k < Z, jnp.exp(l1[k, 0:4].astype(f32)) * state + l1[k, 4:8].astype(f32), state)
 
     mark("gated")
     for b in range(NB):
@@ -523,8 +524,7 @@
     arrived(("r", 4), rb.at[0, pl.ds(2, 2)])
     arrived(("r", 5), rb.at[1, pl.ds(0, 2)])
     mark("final")
-    ob[...] = (mine + rb[0].astype(f32) + rb[1].astype(f32)).astype(bf16)
-    c_out = fetch("out", ob, out_ref)
+    out_ref[...] = (mine + rb[0].astype(f32) + rb[1].astype(f32)).astype(bf16)
 
     mark("drain")
     left(0, tr.at[pl.ds(0, 3)])
@@ -540,8 +540,6 @@
         def _():
             to_group(d).wait_send()
 
-    mark("outwait")
-    c_out.wait()
     assert len(slot.index) <= N_COPIES and len(local.index) <= N_LOCAL
     mark(None)
 
@@ -564,9 +562,9 @@
     return pl.pallas_call(
         kernel,
         name="layer",
-        out_shape=jax.ShapeDtypeStruct((SEQS, TOK, D), bf16),
+        out_shape=pltpu.VMEM((SEQS, TOK, D), bf16),
         in_specs=[hbm] * 12,
-        out_specs=hbm,
+        out_specs=pl.BlockSpec(memory_space=pltpu.VMEM),
         scratch_shapes=[
             pltpu.VMEM((1, D), f32),
             pltpu.VMEM((SEQS, STR, D), bf16),
@@ -576,8 +574,8 @@
             pltpu.VMEM((NB, W, D), bf16),
             pltpu.VMEM((NB, 8, 1, W), f32),
             pltpu.VMEM((NB, ROWS, W), f32),
-            pltpu.VMEM((NB, 32, W), f32),
-            pltpu.VMEM((NB, 32, W), f32),
+            pltpu.VMEM((NB, 32, W), bf16),
+            pltpu.VMEM((NB, 32, W), bf16),
             pltpu.VMEM((ROWS, CH), bf16),
             pltpu.VMEM((2, ROWS, W), f32),
             pltpu.VMEM((NB, ROWS, W), f32),
@@ -593,7 +591,6 @@
             pltpu.VMEM((2, 2, TOK, D), f32),
             pltpu.VMEM((2, 2, TOK, D), bf16),
             pltpu.VMEM((2, SEQS, TOK, D), bf16),
-            pltpu.VMEM((SEQS, TOK, D), bf16),
             pltpu.SemaphoreType.DMA((N_SENDS,)),
             pltpu.SemaphoreType.DMA((N_COPIES,)),
             pltpu.SemaphoreType.DMA((N_LOCAL,)),

time: 49.7 us -> 46.9 us (0.944)
  Pallas kernels: 47.9 us -> 46.1 us
  local copies, waits for them, and re-layouts: 1.67 us -> 0.71 us
    pallas_call x1, Pallas kernels: 47.9 us -> 46.1 us  [per_device(): pl.pallas_call(kernel, name='layer', out_shape=pltpu.VMEM((SEQS, TOK, D),...]
    unnamed x1, local copies, waits for them, and re-layouts: 1.67 us -> 0.71 us
where the time goes in v4:
time: 46.9 us; the launch traced here: 46.8 us
  Pallas kernels  46.1 us (98%)
  local copies, waits for them, and re-layouts  0.71 us (2%)
    pallas_call x1, Pallas kernels, per_device(): pl.pallas_call(kernel, name='layer', out_shape=pltpu.VMEM((SEQS, TOK, D),...  46.1 us

profile of v4, /device:TPU:1, one launch (start us, length us, event | category | flops | bytes accessed | tf_op | source)
XLA Modules:
  0.0 46.8 jit_solution(4750670568883832151)
XLA Ops:
  0.0 46.1 %layer.1 = bf16[4,16,2048]{2,1,0:T(8,128)(2,1)S(1)} custom-call(bf16[4,16,2048]{2,1,0:T(8,128)(2,1)} %tok_ref.1, f32[1,2048]{1,0:T(1,128)} %bitcast.6, bf16[2048,128]{1,0:T(8,128)(2,1)} %w1_ref.1, bf16[2048,128]{1,0:T(8,128)(2,1)} %w2_ref.1, bf16[1,128,128]{2,1,0:T(8,128)(2,1)} %rw_ref.1, bf16[1,128,128]{2,1,0:T(8,128)(2,1)} %ew_ref.1, ...), custom_call_target="tpu_custom_call" | custom-call | tf_op jit(solution)/shard_map/layer/pallas_call | solution.py:562
  46.1 0.7 %copy.14 = bf16[4,16,2048]{2,1,0:T(8,128)(2,1)} copy(bf16[4,16,2048]{2,1,0:T(8,128)(2,1)S(1)} %layer.1) | data formatting | bytes 524288

commit v5 on v4

--- a/solution.py
+++ b/solution.py
@@ -32,9 +32,9 @@
         return self.index.setdefault(key, len(self.index))
 
 
-N_COPIES = 74
+N_COPIES = 44
 N_SENDS = 16
-N_LOCAL = 7
+N_LOCAL = 6
 VMEM_LIMIT = 66700000
 
 
@@ -187,7 +187,11 @@
 
     def piece(m, z, q, core, h):
         rows, base = PIECE[m]
-        k = q * 4 + core * 2 + h
+        k = core * 2 + h
+        if m == 1:
+            rows = 2 * rows
+        else:
+            k = k + q * 4
         place = pl.ds(pl.multiple_of(base + k * rows, 16), rows)
         if m == 3:
             return wog.at[z, place]
@@ -195,57 +199,69 @@
 
     blocks = (mod4(Z - 1), mod4(Z + 1), mod4(Z + 2))
 
-    def own_send(m):
-        for j, h, dev in ((0, 0, zp), (1, 1, zm), (0, 1, zp), (1, 0, zm)):
-            ref = piece(m, Z, par, C, h)
-            send(1 + m, ("z", m, j, h), ref, ref, dev)
-
-    def z_event(m, j, h):
-        ref = piece(m, blocks[j], par, C, h)
-        arrived(("z", m, j, h), ref)
-        if (j, h) == (0, 0):
-            send(1 + m, ("z", m, 2, 0), ref, ref, zp)
-        if (j, h) == (1, 1):
-            send(1 + m, ("z", m, 2, 1), ref, ref, zm)
-        send(1 + m, ("x", m, j, h), ref, ref, xp if h == 0 else xm)
-        send(1 + m, ("d", m), ref, ref, mate)
-
-    def x_event(m, j, h):
-        ref = piece(m, blocks[j], 1 - par, C, h)
-        arrived(("x", m, j, h), ref)
-        send(1 + m, ("d", m), ref, ref, mate)
+    def own_piece(m, j, h):
+        ref = piece(m, Z, par, C, h)
+        send(1 + m, ("z", m, j == h), ref, ref, zm if j else zp)
+
+    def own_first(m):
+        own_piece(m, 0, 0)
+        own_piece(m, 1, 1)
+
+    def own_second(m):
+        own_piece(m, 0, 1)
+        own_piece(m, 1, 0)
+
+    def both(m):
+        return (wa, wa, wv, wog)[m].at[0, pl.ds(0, PIECE[m][0] * (4 if m == 1 else 2))]
+
+    def z_pair(m, pair, key):
+        arrived(("z", m, key), both(m))
+        for j, h in pair:
+            ref = piece(m, blocks[j], par, C, h)
+            if (j, h) == (0, 0):
+                send(1 + m, ("z", m, 2), ref, ref, zp)
+            if (j, h) == (1, 1):
+                send(1 + m, ("z", m, 2), ref, ref, zm)
+        for j, h in pair:
+            ref = piece(m, blocks[j], par, C, h)
+            if m != 1:
+                send(1 + m, ("x", m, key), ref, ref, xp if h == 0 else xm)
+            send(1 + m, ("d", m), ref, ref, mate)
+
+    def x_pair(m, pair, key):
+        arrived(("x", m, key), both(m))
+        for j, h in pair:
+            ref = piece(m, blocks[j], 1 - par, C, h)
+            send(1 + m, ("d", m), ref, ref, mate)
+
+    NEAR, NEXT, FAR = ((0, 0), (1, 1)), ((0, 1), (1, 0)), ((2, 0), (2, 1))
 
     def near_z(m):
-        z_event(m, 0, 0)
-        z_event(m, 1, 1)
+        z_pair(m, NEAR, True)
 
     def next_z(m):
-        z_event(m, 0, 1)
-        z_event(m, 1, 0)
+        z_pair(m, NEXT, False)
 
     def far_z(m):
-        z_event(m, 2, 0)
-        z_event(m, 2, 1)
+        z_pair(m, FAR, 2)
 
     def near_x(m):
-        x_event(m, 0, 0)
-        x_event(m, 1, 1)
+        x_pair(m, NEAR, True)
 
     def next_x(m):
-        x_event(m, 0, 1)
-        x_event(m, 1, 0)
+        x_pair(m, NEXT, False)
 
     def far_x(m):
-        x_event(m, 2, 0)
-        x_event(m, 2, 1)
+        x_pair(m, FAR, 2)
 
     def volume(m, parts):
         return (wa, wa, wv, wog)[m].at[pl.ds(0, parts // 6), pl.ds(0, PIECE[m][0] * 6)]
 
     mark("weights")
     pltpu.make_async_copy(wa.at[0], wa.at[0], lsem.at[local("wa")]).wait()
-    own_send(0)
-    own_send(1)
+    own_first(0)
+    own_second(0)
+    own_first(1)
     pltpu.make_async_copy(sm.at[0], sm.at[0], lsem.at[local("sm")]).wait()
     for d in (1, 2, 3):
         send(5, ("s",), sm.at[Z], sm.at[Z], {"z": mod4(Z + d)})
@@ -264,29 +280,32 @@
     norm(Y, 1)
     mark("net0")
     near_z(0)
-    near_z(1)
-    c_wv.wait()
-    own_send(2)
-    c_wo.wait()
-    own_send(3)
+    own_second(1)
     mark("net1")
+    next_z(0)
+    mark("net1t")
     arrived(("t", 0, 0), tok(y_m, 0))
     send(0, ("t", 2, 0), tok(y_m, 0), tok(y_m, 0), yp)
     arrived(("t", 1, 1), tok(y_p, 1))
     send(0, ("t", 2, 1), tok(y_p, 1), tok(y_p, 1), ym)
     mark("net2")
-    next_z(0)
-    next_z(1)
+    near_z(1)
+    c_wv.wait()
+    own_first(2)
+    own_second(2)
+    c_wo.wait()
+    own_first(3)
+    own_second(3)
     mark("norm1")
     norm(y_m, 0)
     norm(y_p, 1)
     mark("net3")
+    far_z(0)
+    mark("net3a")
     near_x(0)
-    near_x(1)
-    far_z(0)
-    far_z(1)
     next_x(0)
-    next_x(1)
+    mark("net3b")
+    next_z(1)
     mark("net3t")
     arrived(("t", 0, 1), tok(y_m, 1))
     arrived(("t", 1, 0), tok(y_p, 0))
@@ -294,10 +313,9 @@
     norm(y_m, 1)
     norm(y_p, 0)
     mark("net4")
-    near_z(2)
+    far_z(1)
     mark("net5")
     far_x(0)
-    far_x(1)
     mark("net5t")
     arrived(("t", 2, 0), tok(y_d, 0))
     norm(y_d, 0)
@@ -323,9 +341,7 @@
                 hs[n, s * 8 : s * 8 + 8, :] = last.astype(bf16)
     send(6, ("h",), hs, hr, nxt)
     mark("net6")
-    next_z(2)
-    near_z(3)
-    near_x(2)
+    near_z(2)
     arrived(("s",), sm.at[pl.ds(0, 3)])
 
     mark("conv")
@@ -369,10 +385,8 @@
             de[b, rows, :], pu[b, rows, :] = gates(b, lg[0, rows, :], lg[1, rows, :], cv[rows, cols])
 
     mark("net7")
-    next_z(3)
-    next_x(2)
-    far_z(2)
-    near_x(3)
+    next_z(2)
+    near_z(3)
     mark("halo")
     arrived(("h",), hr)
     mark("redo")
@@ -427,12 +441,15 @@
         s_own[:, cols] = jnp.concatenate(tot_a + tot_h, axis=0).astype(bf16)
 
     mark("states")
-    for d in (1, 2, 3):
+    for d in (2, 1, 3):
         send(7, ("e",), s_own, l1.at[Z], {"z": mod4(Z + d)})
     l1[Z] = s_own[...]
+    near_x(2)
+    next_z(3)
+    far_z(2)
+    next_x(2)
+    near_x(3)
     far_z(3)
-    next_x(3)
-    far_x(2)
     mark("states1")
     arrived(("e",), l1.at[pl.ds(0, 3)])
     total_a, total_h = l1[0, 0:4].astype(f32), l1[0, 4:8].astype(f32)
@@ -445,14 +462,15 @@
     def to_group(d):
         return remote(8 + d, ("g", d), t_own, l2.at[g], gdev(lax.rem(g + d, 8)))
 
-    for d in range(1, 8):
+    for d in (4, 5, 3, 2, 6, 7, 1):
 
         @pl.when(g + d < 8)
         def _():
             to_group(d).start()
 
     mark("net8")
-    far_x(3)
+    far_x(2)
+    mark("net8d")
     arrived(("d", 2), volume(2, 12))
     mark("valve")
     for b in range(0, NB, 2):
@@ -460,6 +478,9 @@
         v = v / (1.0 + jnp.exp(-v))
         sg[b] = v[:, 0:W]
         sg[b + 1] = v[:, W : 2 * W]
+    mark("net9")
+    next_x(3)
+    far_x(3)
     mark("states2")
     for d in range(1, 8):
 
@@ -508,21 +529,18 @@
     pf[1] = p[2:4]
     p = product(y_m).reshape(SEQS, TOK, D)
     pb[2, 2:4] = p[2:4].astype(bf16)
-    send(8, ("r", 3), pb.at[2, pl.ds(2, 2)], rb.at[1, pl.ds(2, 2)], ym)
+    send(8, ("r", 2), pb.at[2, pl.ds(2, 2)], rb.at[1, pl.ds(2, 2)], ym)
     pf[0] = p[0:2]
     mine = product(Y).reshape(SEQS, TOK, D)
     mark("red1")
     arrived(("r", 1), rd.at[1])
     pb[1, 2:4] = (pf[1] + rd[1].astype(f32)).astype(bf16)
-    send(8, ("r", 4), pb.at[1, pl.ds(2, 2)], rb.at[0, pl.ds(2, 2)], yp)
+    send(8, ("r", 2), pb.at[1, pl.ds(2, 2)], rb.at[0, pl.ds(2, 2)], yp)
     arrived(("r", 0), rd.at[0])
     pb[2, 0:2] = (pf[0] + rd[0].astype(f32)).astype(bf16)
-    send(8, ("r", 5), pb.at[2, pl.ds(0, 2)], rb.at[1, pl.ds(0, 2)], ym)
+    send(8, ("r", 2), pb.at[2, pl.ds(0, 2)], rb.at[1, pl.ds(0, 2)], ym)
     mark("red2")
-    arrived(("r", 2), rb.at[0, pl.ds(0, 2)])
-    arrived(("r", 3), rb.at[1, pl.ds(2, 2)])
-    arrived(("r", 4), rb.at[0, pl.ds(2, 2)])
-    arrived(("r", 5), rb.at[1, pl.ds(0, 2)])
+    arrived(("r", 2), rb)
     mark("final")
     out_ref[...] = (mine + rb[0].astype(f32) + rb[1].astype(f32)).astype(bf16)
 
@@ -540,7 +558,7 @@
         def _():
             to_group(d).wait_send()
 
-    assert len(slot.index) <= N_COPIES and len(local.index) <= N_LOCAL
+    assert len(slot.index) == N_COPIES and len(local.index) == N_LOCAL
     mark(None)
 
 

time: 46.9 us -> 45.5 us (0.970)
  Pallas kernels: 46.1 us -> 44.7 us
    pallas_call x1, Pallas kernels: 46.1 us -> 44.7 us  [per_device(): pl.pallas_call(kernel, name='layer', out_shape=pltpu.VMEM((SEQS, TOK, D),...]
where the time goes in v5:
time: 45.5 us; the launch traced here: 45.4 us
  Pallas kernels  44.7 us (98%)
  local copies, waits for them, and re-layouts  0.71 us (2%)
    pallas_call x1, Pallas kernels, per_device(): pl.pallas_call(kernel, name='layer', out_shape=pltpu.VMEM((SEQS, TOK, D),...  44.7 us

profile of v5, /device:TPU:1, one launch (start us, length us, event | category | flops | bytes accessed | tf_op | source)
XLA Modules:
  0.0 45.4 jit_solution(13423108512145927877)
XLA Ops:
  0.0 44.7 %layer.1 = bf16[4,16,2048]{2,1,0:T(8,128)(2,1)S(1)} custom-call(bf16[4,16,2048]{2,1,0:T(8,128)(2,1)} %tok_ref.1, f32[1,2048]{1,0:T(1,128)} %bitcast.6, bf16[2048,128]{1,0:T(8,128)(2,1)} %w1_ref.1, bf16[2048,128]{1,0:T(8,128)(2,1)} %w2_ref.1, bf16[1,128,128]{2,1,0:T(8,128)(2,1)} %rw_ref.1, bf16[1,128,128]{2,1,0:T(8,128)(2,1)} %ew_ref.1, ...), custom_call_target="tpu_custom_call" | custom-call | tf_op jit(solution)/shard_map/layer/pallas_call | solution.py:580
  44.7 0.7 %copy.14 = bf16[4,16,2048]{2,1,0:T(8,128)(2,1)} copy(bf16[4,16,2048]{2,1,0:T(8,128)(2,1)S(1)} %layer.1) | data formatting | bytes 524288

commit v6 on v5

--- a/solution.py
+++ b/solution.py
@@ -19,7 +19,7 @@
 CH = NB * W
 ROWS = SEQS * STR
 AROWS = D + 2 * W
-PIECE = ((AROWS // 16, 0), (AROWS // 16, AROWS // 2), (D // 8, 0), (W // 8, 0))
+PIECE = ((AROWS // 12, 0), (AROWS // 24, AROWS * 2 // 3), (D // 8, 0), (W // 8, 0))
 f32 = jnp.float32
 bf16 = jnp.bfloat16
 

time: 45.5 us -> 47.4 us (1.042)
  Pallas kernels: 44.7 us -> 46.6 us
    pallas_call x1, Pallas kernels: 44.7 us -> 46.6 us  [per_device(): pl.pallas_call(kernel, name='layer', out_shape=pltpu.VMEM((SEQS, TOK, D),...]
where the time goes in v6:
time: 47.4 us; the launch traced here: 47.3 us
  Pallas kernels  46.6 us (98%)
  local copies, waits for them, and re-layouts  0.71 us (1%)
    pallas_call x1, Pallas kernels, per_device(): pl.pallas_call(kernel, name='layer', out_shape=pltpu.VMEM((SEQS, TOK, D),...  46.6 us

profile of v6, /device:TPU:1, one launch (start us, length us, event | category | flops | bytes accessed | tf_op | source)
XLA Modules:
  0.0 47.3 jit_solution(17067434713188486474)
XLA Ops:
  0.0 46.6 %layer.1 = bf16[4,16,2048]{2,1,0:T(8,128)(2,1)S(1)} custom-call(bf16[4,16,2048]{2,1,0:T(8,128)(2,1)} %tok_ref.1, f32[1,2048]{1,0:T(1,128)} %bitcast.6, bf16[2048,128]{1,0:T(8,128)(2,1)} %w1_ref.1, bf16[2048,128]{1,0:T(8,128)(2,1)} %w2_ref.1, bf16[1,128,128]{2,1,0:T(8,128)(2,1)} %rw_ref.1, bf16[1,128,128]{2,1,0:T(8,128)(2,1)} %ew_ref.1, ...), custom_call_target="tpu_custom_call" | custom-call | tf_op jit(solution)/shard_map/layer/pallas_call | solution.py:580
  46.6 0.7 %copy.14 = bf16[4,16,2048]{2,1,0:T(8,128)(2,1)} copy(bf16[4,16,2048]{2,1,0:T(8,128)(2,1)S(1)} %layer.1) | data formatting | bytes 524288

commit v7 on v6

--- a/solution.py
+++ b/solution.py
@@ -19,7 +19,7 @@
 CH = NB * W
 ROWS = SEQS * STR
 AROWS = D + 2 * W
-PIECE = ((AROWS // 12, 0), (AROWS // 24, AROWS * 2 // 3), (D // 8, 0), (W // 8, 0))
+PIECE = ((AROWS // 24, 0), (AROWS // 12, AROWS // 3), (D // 8, 0), (W // 8, 0))
 f32 = jnp.float32
 bf16 = jnp.bfloat16
 

time: 47.4 us -> 45.8 us (0.966)
  Pallas kernels: 46.6 us -> 44.9 us
    pallas_call x1, Pallas kernels: 46.6 us -> 44.9 us  [per_device(): pl.pallas_call(kernel, name='layer', out_shape=pltpu.VMEM((SEQS, TOK, D),...]
where the time goes in v7:
time: 45.8 us; the launch traced here: 45.7 us
  Pallas kernels  44.9 us (98%)
  local copies, waits for them, and re-layouts  0.71 us (2%)
    pallas_call x1, Pallas kernels, per_device(): pl.pallas_call(kernel, name='layer', out_shape=pltpu.VMEM((SEQS, TOK, D),...  44.9 us

profile of v7, /device:TPU:1, one launch (start us, length us, event | category | flops | bytes accessed | tf_op | source)
XLA Modules:
  0.0 45.7 jit_solution(10105815575824398021)
XLA Ops:
  0.0 44.9 %layer.1 = bf16[4,16,2048]{2,1,0:T(8,128)(2,1)S(1)} custom-call(bf16[4,16,2048]{2,1,0:T(8,128)(2,1)} %tok_ref.1, f32[1,2048]{1,0:T(1,128)} %bitcast.6, bf16[2048,128]{1,0:T(8,128)(2,1)} %w1_ref.1, bf16[2048,128]{1,0:T(8,128)(2,1)} %w2_ref.1, bf16[1,128,128]{2,1,0:T(8,128)(2,1)} %rw_ref.1, bf16[1,128,128]{2,1,0:T(8,128)(2,1)} %ew_ref.1, ...), custom_call_target="tpu_custom_call" | custom-call | tf_op jit(solution)/shard_map/layer/pallas_call | solution.py:580
  45.0 0.7 %copy.14 = bf16[4,16,2048]{2,1,0:T(8,128)(2,1)} copy(bf16[4,16,2048]{2,1,0:T(8,128)(2,1)S(1)} %layer.1) | data formatting | bytes 524288
